TPU v7x, 512 devices: a whole 4x4x16 slice. The times are simulated.
512 devices in a mesh: sp: 64 (over z, y), tp: 8 (over x, core).
Axes of the slice: x: 4, y: 4, z: 16, core: 2. Of those that a mesh axis runs over, the one named last changes fastest.
Arguments:
- prompt: bfloat16 [8, 4096, 2048], P(None, 'sp'), may hold values from -6 to 6
- keep_scale: float32 [8, 4096], P(None, 'sp'), may hold values from 0.25 to 1
- new_token: bfloat16 [8, 2048], P(None, 'tp'), may hold values from -6 to 6
- w_query: bfloat16 [2048, 1024], P(None, 'tp'), may hold values from -0.125 to 0.125
- w_forget: bfloat16 [2048, 1024], P(None, 'tp'), may hold values from -0.125 to 0.125
- w_value: bfloat16 [2048, 1024], P(None, 'tp'), may hold values from -4.21875 to 4.21875
- w_outgate: bfloat16 [2048, 1024], P(None, 'tp'), may hold values from -0.125 to 0.125
- floor_gap: float32 [1024], P('tp'), may hold values from 0 to 0.06
- norm_gain: float32 [128], replicated, may hold values from 0.1 to 1.9
Outputs:
- state_cache: bfloat16 [8, 1024, 128], P('tp', 'sp')
- first_read: bfloat16 [8, 1024], P(None, 'tp')
All inputs are finite; a program needn't handle non-finite values.
Results may differ from a plain program's by a relative error of at most 0.0022.
The roundings to bfloat16 on the way count: a program that leaves them out, or rounds other values in their place, can miss the bound.
Values may be sent and summed in bfloat16 or wider, within the bound.
No kernel may reach another device: no remote copies, remote signals or barrier semaphores. Data moves between devices by JAX's collectives and lax.ppermute only.
A program may use at most 64 MiB of HBM per device.

v0:
```python
import functools

import jax
import jax.numpy as jnp
from jax import lax
from jax.sharding import Mesh
from jax.sharding import PartitionSpec as P

SP = ("sp_0", "sp_1")


HIGHEST_PRECISION = lax.Precision.HIGHEST
EPSILON = 1e-06


def copy_for_each(x, axis):
    length = lax.axis_size(axis)
    return lax.all_to_all(jnp.broadcast_to(x[None], (length, *x.shape)), axis, 0, 0, tiled=True)


def combined_pairwise(pieces, combine):
    while len(jax.tree.leaves(pieces)[0]) > 1:
        pieces = jax.vmap(combine)(*(pieces[side::2] for side in (0, 1)))
    return pieces[0]


def entering(x, axis, combine, identity):
    length, index = (lax.axis_size(axis), lax.axis_index(axis))
    passed = jnp.arange(length) > index

    def kept(part, zero, own):
        part = jnp.where(
            passed.reshape(-1, *(1 for _ in own.shape)), part, jnp.asarray(zero, own.dtype)
        )
        return part[::-1]

    pieces = copy_for_each(x, axis)
    return combined_pairwise(kept(pieces, identity, x), combine)


def split_up(x, dim, length):
    shape = x.shape
    blocks = x.reshape(*shape[:dim], length, shape[dim] // length, *shape[dim + 1 :])
    return jnp.moveaxis(blocks, dim, 0)


def summed_on_arrival(x, axis, dim):
    length = lax.axis_size(axis)
    blocks = lax.all_to_all(split_up(x, dim, length), axis, 0, 0, tiled=True)
    return jnp.sum(blocks, axis=0)


def joined_along(blocks, dim):
    shape = list(blocks.shape[1:])
    shape[dim] *= blocks.shape[0]
    return jnp.moveaxis(blocks, 0, dim).reshape(shape)


def gathered_copies(x, axis, dim):
    blocks = copy_for_each(x, axis)
    return joined_along(blocks, dim)


def by_axis(x, axes):
    return functools.reduce(lax.psum, axes, x)


def add_totals(earlier, following):
    return earlier + following


def later_totals(block_log):
    return entering(block_log, SP, add_totals, jnp.zeros_like(block_log))


def per_device(
    prompt, keep_scale, new_token, w_query, w_forget, w_value, w_outgate, floor_gap, norm_gain
):
    sequences, positions, model_width = prompt.shape
    head_size = norm_gain.shape[0]
    local_heads = w_forget.shape[1] // head_size
    flattened = prompt.reshape(sequences * positions, model_width)
    forget_pre = jnp.dot(flattened, w_forget, preferred_element_type=jnp.float32)
    forget_pre = forget_pre.reshape(sequences, positions, local_heads, head_size)
    values = jnp.dot(flattened, w_value, preferred_element_type=jnp.float32).astype(jnp.bfloat16)
    values = lax.optimization_barrier(values).astype(jnp.float32)
    values = values.reshape(sequences, positions, local_heads, head_size)
    floor_rows = floor_gap.reshape(local_heads, head_size)
    forget_loss = floor_rows * (1.0 - jax.nn.sigmoid(forget_pre))
    keep_factor = keep_scale[:, :, None, None]
    log_forget = jnp.log(keep_factor) + jnp.log1p(-forget_loss)
    input_gate = 1.0 - keep_factor + keep_factor * forget_loss
    inside_log = lax.cumsum(log_forget, axis=1, reverse=True) - log_forget
    block_log = jnp.sum(log_forget, axis=1).transpose(1, 0, 2)
    states = jnp.einsum(
        "sthc,sthv->hscv", input_gate * jnp.exp(inside_log), values, precision=HIGHEST_PRECISION
    )
    later_log = None
    later_log = later_totals(block_log)
    decayed = states * jnp.exp(later_log)[..., None]
    final_rows = summed_on_arrival(
        decayed.reshape(local_heads, sequences * head_size, head_size), SP, 1
    )
    weights = (w_query, w_forget, w_value, w_outgate)
    portion = gathered_copies(new_token, "tp", 1)
    query, new_forget, new_value, new_gate = tuple(
        (jnp.dot(portion, weight, preferred_element_type=jnp.float32) for weight in weights)
    )
    shaped = (sequences, local_heads, head_size)
    new_value = (
        lax.optimization_barrier(new_value.astype(jnp.bfloat16)).astype(jnp.float32).reshape(shaped)
    )
    query = query.reshape(shaped)
    new_forget = new_forget.reshape(shaped)
    new_gate = new_gate.reshape(shaped)
    new_loss = floor_rows * (1.0 - jax.nn.sigmoid(new_forget))
    read_weight = (query * (1.0 - new_loss)).transpose(1, 0, 2)
    read_part = jnp.einsum(
        "hsc,hscv->hsv", read_weight * jnp.exp(later_log), states, precision=HIGHEST_PRECISION
    )
    mixed_read = by_axis(read_part, SP).transpose(1, 0, 2)
    own_term = jnp.sum(query * new_loss, axis=-1, keepdims=True)
    mixed_read = mixed_read + own_term * new_value
    normed = mixed_read * lax.rsqrt(
        jnp.mean(mixed_read * mixed_read, axis=-1, keepdims=True) + EPSILON
    )
    first_read = (normed * norm_gain * jax.nn.silu(new_gate)).reshape(
        sequences, local_heads * head_size
    )
    return (final_rows.astype(jnp.bfloat16), first_read.astype(jnp.bfloat16))


def solution(mesh):
    finer = Mesh(mesh.devices.reshape(16, 4, mesh.shape["tp"]), ("sp_0", "sp_1", "tp"))
    placed = (
        P(None, SP, None),
        P(None, SP),
        P(None, "tp"),
        P(None, "tp"),
        P(None, "tp"),
        P(None, "tp"),
        P(None, "tp"),
        P("tp"),
        P(),
    )
    return jax.shard_map(
        per_device,
        mesh=finer,
        in_specs=placed,
        out_specs=(P("tp", SP, None), P(None, "tp")),
        check_vma=False,
    )
```

profile of v0, /device:TPU:2, one launch (start us, length us, event | category | flops | bytes accessed | tf_op | source)
XLA Modules:
  0.0 122.2 jit_solution(5089082918941294203)
XLA Ops:
  0.6 0.0 copy-start
  0.6 1.4 %broadcast_in_dim.19 = bf16[8,8,256]{2,1,0:T(8,128)(2,1)} broadcast(bf16[8,256]{1,0:T(8,128)(2,1)} %param.11), dimensions={1,2} | broadcast | bytes 36864 | tf_op jit(solution)/shard_map/broadcast_in_dim | solution.py:18
  2.1 9.1 %all-to-all-start.2 = ((bf16[8,8,256]{2,1,0:T(8,128)(2,1)}), bf16[8,8,256]{2,1,0:T(8,128)(2,1)S(1)}, u32[]{:S(2)}, u32[]{:S(2)}) async-start(bf16[8,8,256]{2,1,0:T(8,128)(2,1)} %broadcast_in_dim.19), calls=%async_computation.2 | async-start | bytes 65536 | tf_op jit(solution)/shard_map/all_to_all | solution.py:18
  11.2 0.7 broadcast_subtract_fusion
  11.9 0.0 copy-done
  11.9 2.7 %fusion.21 = (f32[8,128]{1,0:T(8,128)S(1)}, f32[8,64,128]{2,1,0:T(8,128)}, f32[8,64,128]{2,1,0:T(8,128)}) fusion(f32[8,64]{1,0:T(8,128)S(1)} %get-tuple-element.10, bf16[8,64,2048]{2,1,0:T(8,128)(2,1)S(1)} %copy-done, bf16[2048,128]{1,0:T(8,128)(2,1)} %param.13, f32[128]{0:T(128)} %param.16), kind=kOutput, calls=%fused_computation.30 | convolution fusion | flops 268958720 | bytes 3152384 | tf_op jit(solution)/shard_map/dot_general | solution.py:83
  14.6 0.7 all-to-all-done.2
  15.2 0.7 broadcast_in_dim.17
  15.9 14.4 %all-to-all-start = ((f32[64,1,8,128]{3,2,1,0:T(8,128)}), f32[64,1,8,128]{3,2,1,0:T(8,128)S(1)}, u32[]{:S(2)}, u32[]{:S(2)}) async-start(f32[64,1,8,128]{3,2,1,0:T(8,128)} %broadcast_in_dim.17), calls=%async_computation | async-start | bytes 524288 | tf_op jit(solution)/shard_map/all_to_all | solution.py:18
  30.4 0.0 copy-done.1
  30.4 1.4 %convolution_convert_fusion = bf16[512,128]{1,0:T(8,128)(2,1)} fusion(bf16[512,2048]{1,0:T(8,128)(2,1)S(1)} %bitcast.40, bf16[2048,128]{1,0:T(8,128)(2,1)S(1)} %copy-done.1), kind=kOutput, calls=%fused_computation.6 | convolution fusion | flops 268500992 | bytes 2752512 | tf_op jit(solution)/shard_map/dot_general | solution.py:85
  31.7 1.3 %fusion.15 = f32[8,64,128]{2,0,1:T(8,128)S(1)} fusion(f32[8,64,128]{2,1,0:T(8,128)} %get-tuple-element.5), kind=kOutput, calls=%fused_computation.19 | output fusion | flops 4128768 | bytes 524288 | tf_op jit(solution)/shard_map/per_device/reduce_window_sum | solution.py:93
  33.1 0.0 copy-done.2
  33.1 0.2 fusion.26
  33.3 19.5 %all-to-all-done = f32[64,1,8,128]{3,2,1,0:T(8,128)S(1)} async-done(((f32[64,1,8,128]{3,2,1,0:T(8,128)}), f32[64,1,8,128]{3,2,1,0:T(8,128)S(1)}, u32[]{:S(2)}, u32[]{:S(2)}) %all-to-all-start) | async-done | bytes 262176 | tf_op jit(solution)/shard_map/all_to_all | solution.py:18
  52.7 0.1 broadcast_select_fusion
  53.0 0.0 copy-done.5
  53.0 1.3 %multiply_multiply_fusion = (f32[8,128]{1,0:T(8,128)S(1)}, f32[8,128]{1,0:T(8,128)S(1)}, f32[8]{0:T(128)S(1)}) fusion(f32[8,128]{1,0:T(8,128)S(1)} %fusion.26, f32[2,1,8,128]{3,2,1,0:T(8,128)S(1)} %slice_add_fusion.3, bf16[8,2048]{1,0:T(8,128)(2,1)S(1)} %bitcast.42, bf16[2048,128]{1,0:T(8,128)(2,1)} %param.13, f32[128]{0:T(128)S(1)} %copy-done.5), kind=kOutput, calls=%fused_computation.41 | convolution fusion | flops 4205560 | bytes 578080 | tf_op jit(solution)/shard_map/dot_general | solution.py:107
  54.3 0.0 copy-start.6
  54.3 0.0 copy-done.4
  54.4 0.0 copy-done.3
  54.4 2.6 %broadcast_multiply_fusion = (f32[8,128,128]{2,1,0:T(8,128)}, f32[8,128,128]{2,1,0:T(8,128)S(1)}) fusion(f32[8,128]{1,0:T(8,128)S(1)} %get-tuple-element.3, bf16[8,64,128]{2,1,0:T(8,128)(2,1)S(1)} %bitcast.45, f32[8,64,128]{2,0,1:T(8,128)S(1)} %fusion.15, f32[8,64,128]{2,1,0:T(8,128)} %get-tuple-element.11, f32[8,64]{1,0:T(8,128)S(1)} %copy-done.4, ...), kind=kOutput, calls=%fused_computation.21 | convolution fusion | flops 101187584 | bytes 1714176 | tf_op jit(solution)/shard_map/sthc,sthv->hscv/dot_general | solution.py:95
  57.0 5.0 %all-to-all-start.1 = ((f32[64,1,16,128]{3,2,1,0:T(8,128)}), f32[64,1,16,128]{3,2,1,0:T(8,128)S(1)}, u32[]{:S(2)}, u32[]{:S(2)}) async-start(f32[64,1,16,128]{3,2,1,0:T(8,128)} %bitcast.5), calls=%async_computation.1 | async-start | bytes 1048576 | tf_op jit(solution)/shard_map/all_to_all | solution.py:49
  62.0 1.2 convolution_convert_fusion.1
  63.2 0.5 fusion.27
  63.7 45.4 %psum.14 = f32[1,8,128]{2,1,0:T(8,128)S(1)} all-reduce(f32[1,8,128]{2,1,0:T(8,128)S(1)} %bitcast.47), channel_id=1, replica_groups=mesh['sp_0'=16,'sp_1'=4,'tp'=8] {'sp_0'}, use_global_device_ids=true, to_apply=%region_3.4 | all-reduce | flops 1024 | bytes 8192 | tf_op jit(solution)/shard_map/psum | solution.py:65
  109.1 10.4 %psum.15 = f32[8,128]{1,0:T(8,128)S(1)} all-reduce(f32[8,128]{1,0:T(8,128)S(1)} %bitcast.48), channel_id=1, replica_groups=mesh['sp_0'=16,'sp_1'=4,'tp'=8] {'sp_1'}, use_global_device_ids=true, to_apply=%region_4.5 | all-reduce | flops 1024 | bytes 8192 | tf_op jit(solution)/shard_map/psum | solution.py:65
  119.5 0.2 multiply_reduce_fusion
  119.7 0.0 copy-done.6
  119.7 1.8 %multiply_convert_fusion = bf16[8,128]{1,0:T(8,128)(2,1)} fusion(f32[8,128]{1,0:T(8,128)S(1)} %psum.15, bf16[8,128]{1,0:T(8,128)(2,1)S(1)} %convolution_convert_fusion.1, f32[128]{0:T(128)S(1)} %copy-done.6, f32[8]{0:T(128)S(1)} %add_rsqrt_fusion, f32[8]{0:T(128)S(1)} %get-tuple-element.8, bf16[8,2048]{1,0:T(8,128)(2,1)S(1)} %bitcast.44, ...), kind=kOutput, calls=%fused_computation.37 | convolution fusion | flops 4205568 | bytes 565824 | tf_op jit(solution)/shard_map/dot_general | solution.py:107
  121.5 0.0 all-to-all-done.1
  121.5 0.7 reduce_sum.37
  (13 shorter events, 0.1 us)
Async XLA Ops:
  0.6 11.3 %copy-start = (bf16[8,64,2048]{2,1,0:T(8,128)(2,1)S(1)}, bf16[8,64,2048]{2,1,0:T(8,128)(2,1)}, u32[]{:S(2)}) copy-start(bf16[8,64,2048]{2,1,0:T(8,128)(2,1)} %param.9) | copy-start | bytes 6291460
  2.1 13.1 %all-to-all-start.2 = ((bf16[8,8,256]{2,1,0:T(8,128)(2,1)}), bf16[8,8,256]{2,1,0:T(8,128)(2,1)S(1)}, u32[]{:S(2)}, u32[]{:S(2)}) async-start(bf16[8,8,256]{2,1,0:T(8,128)(2,1)} %broadcast_in_dim.19), calls=%async_computation.2 | async-start | bytes 65536 | tf_op jit(solution)/shard_map/all_to_all | solution.py:18
  11.9 18.5 %copy-start.1 = (bf16[2048,128]{1,0:T(8,128)(2,1)S(1)}, bf16[2048,128]{1,0:T(8,128)(2,1)}, u32[]{:S(2)}) copy-start(bf16[2048,128]{1,0:T(8,128)(2,1)} %param.14) | copy-start | bytes 1572868
  14.5 18.5 %copy-start.2 = (bf16[2048,128]{1,0:T(8,128)(2,1)S(1)}, bf16[2048,128]{1,0:T(8,128)(2,1)}, u32[]{:S(2)}) copy-start(bf16[2048,128]{1,0:T(8,128)(2,1)} %param.12) | copy-start | bytes 1572868
  15.9 36.8 %all-to-all-start = ((f32[64,1,8,128]{3,2,1,0:T(8,128)}), f32[64,1,8,128]{3,2,1,0:T(8,128)S(1)}, u32[]{:S(2)}, u32[]{:S(2)}) async-start(f32[64,1,8,128]{3,2,1,0:T(8,128)} %broadcast_in_dim.17), calls=%async_computation | async-start | bytes 524288 | tf_op jit(solution)/shard_map/all_to_all | solution.py:18
  31.7 21.2 %copy-start.5 = (f32[128]{0:T(128)S(1)}, f32[128]{0:T(128)}, u32[]{:S(2)}) copy-start(f32[128]{0:T(128)} %param.16) | copy-start | bytes 1540
  31.7 22.6 %copy-start.4 = (f32[8,64]{1,0:T(8,128)S(1)}, f32[8,64]{1,0:T(8,128)}, u32[]{:S(2)}) copy-start(f32[8,64]{1,0:T(8,128)} %param.10) | copy-start | bytes 6148
  33.3 21.1 %copy-start.3 = (bf16[512,128]{1,0:T(8,128)(2,1)S(1)}, bf16[512,128]{1,0:T(8,128)(2,1)}, u32[]{:S(2)}) copy-start(bf16[512,128]{1,0:T(8,128)(2,1)} %convolution_convert_fusion) | copy-start | bytes 393220
  54.3 65.4 %copy-start.6 = (f32[128]{0:T(128)S(1)}, f32[128]{0:T(128)}, u32[]{:S(2)}) copy-start(f32[128]{0:T(128)} %param.17) | copy-start | bytes 1540
  57.0 64.6 %all-to-all-start.1 = ((f32[64,1,16,128]{3,2,1,0:T(8,128)}), f32[64,1,16,128]{3,2,1,0:T(8,128)S(1)}, u32[]{:S(2)}, u32[]{:S(2)}) async-start(f32[64,1,16,128]{3,2,1,0:T(8,128)} %bitcast.5), calls=%async_computation.1 | async-start | bytes 1048576 | tf_op jit(solution)/shard_map/all_to_all | solution.py:49
where the time goes:
time: 123 us; the launch traced here: 122 us
  blocking collectives  55.8 us (45%)
  starting transfers between devices  28.5 us (23%)
  waiting for transfers between devices  20.1 us (16%)
  matrix products  11.7 us (10%)
  other arithmetic  3.03 us (2%)
  local copies, waits for them, and re-layouts  2.21 us (2%)
    psum x2, blocking collectives, by_axis(): return functools.reduce(lax.psum, axes, x)  55.8 us
    all_to_all x2, starting transfers between devices, copy_for_each(): lax.all_to_all(jnp.broadcast_to(x[None], (length, *x.shape)), axis, 0, 0,...  23.5 us
    all_to_all x2, waiting for transfers between devices, copy_for_each(): lax.all_to_all(jnp.broadcast_to(x[None], (length, *x.shape)), axis, 0, 0,...  20.1 us
    all_to_all x1, starting transfers between devices, summed_on_arrival(): blocks = lax.all_to_all(split_up(x, dim, length), axis, 0, 0, tiled=True)  4.99 us
    dot_general x4, matrix products, per_device(): jnp.dot(portion, weight, preferred_element_type=jnp.float32)  4.57 us
    dot_general x1, matrix products, per_device(): jnp.dot(flattened, w_forget, preferred_element_type=jnp.float32)  2.66 us
    dot_general x1, matrix products, per_device(): jnp.einsum('sthc,sthv->hscv', input_gate * jnp.exp(inside_log), values, p...  2.62 us
  transfers between devices with their start and end apart: 3, of which 2 were waited for; matrix products, arithmetic and copies ran while one was open for 8% of the time, Pallas kernels for 0%

commit v1 on v0

v1 whole, which is shorter than its diff:
```python
import functools

import jax
import jax.numpy as jnp
from jax import lax
from jax.experimental import pallas as pl
from jax.experimental.pallas import tpu as pltpu
from jax.sharding import Mesh
from jax.sharding import PartitionSpec as P

HI, LO, Y, TP = "sp_hi", "sp_lo", "sp_y", "tp"
SP = (HI, LO, Y)
NEAR = (LO, Y)
EPSILON = 1e-06
F32, BF16 = jnp.float32, jnp.bfloat16


def in_three(x):
    high = x.astype(BF16)
    rest = x - high.astype(F32)
    middle = rest.astype(BF16)
    return high, middle, (rest - middle.astype(F32)).astype(BF16)


def state_kernel(
    prompt_ref, keep_ref, gap_ref, wf_ref, wv_ref, out_ref, x_buf, w_buf, p_sem, w_sem
):
    sequences, positions, width = prompt_ref.shape
    head = gap_ref.shape[1]
    peers = out_ref.shape[0]
    rows = head // peers
    pair = 2 * positions
    weights = [
        pltpu.make_async_copy(ref, w_buf.at[:, pl.ds(k * head, head)], w_sem.at[k])
        for k, ref in enumerate((wf_ref, wv_ref))
    ]
    chunks = [
        pltpu.make_async_copy(
            prompt_ref.at[pl.ds(2 * n, 2)], x_buf.at[pl.ds(2 * n, 2)], p_sem.at[n]
        )
        for n in range(sequences // 2)
    ]
    for copy in (*weights, *chunks):
        copy.start()
    keep = keep_ref[...]
    filler = jnp.ones((sequences, head - positions), F32)
    keep_columns = jnp.transpose(jnp.concatenate([keep, filler], axis=1))[:positions]
    log_columns = jnp.log(keep_columns)
    row = lax.broadcasted_iota(jnp.int32, (pair, pair), 0)
    column = lax.broadcasted_iota(jnp.int32, (pair, pair), 1)
    later_mask = (column > row) & (column // positions == row // positions)
    later_mask = later_mask.astype(F32).astype(BF16)
    gap = gap_ref[...]

    def spread(columns, n):
        return jnp.concatenate(
            [
                jnp.broadcast_to(columns[:, s : s + 1], (positions, head))
                for s in (2 * n, 2 * n + 1)
            ],
            axis=0,
        )

    for copy in weights:
        copy.wait()
    for n, copy in enumerate(chunks):
        copy.wait()
        x = x_buf[pl.ds(2 * n, 2)].reshape(pair, width)
        both = jnp.dot(x, w_buf[...], preferred_element_type=F32)
        values = both[:, head:].astype(BF16)
        loss = gap * jax.nn.sigmoid(-both[:, :head])
        keep_factor = spread(keep_columns, n)
        log_forget = spread(log_columns, n) + jnp.log1p(-loss)
        gate = (1.0 - keep_factor) + keep_factor * loss
        later = sum(
            jnp.dot(later_mask, part, preferred_element_type=F32)
            for part in in_three(log_forget)
        )
        gated = in_three(gate * jnp.exp(later))
        for k in range(2):
            s = 2 * n + k
            span = slice(k * positions, (k + 1) * positions)
            left = jnp.concatenate([part[span] for part in gated], axis=0)
            right = jnp.concatenate([values[span]] * 3, axis=0)
            state = lax.dot_general(
                left, right, (((0,), (0,)), ((), ())), preferred_element_type=F32
            )
            first = k * positions
            total = later[first : first + 1] + log_forget[first : first + 1]
            for j in range(peers):
                out_ref[j, s * rows : (s + 1) * rows, :] = state[j * rows : (j + 1) * rows]
                out_ref[j, head + s : head + s + 1, :] = total


def near_kernel(in_ref, out_ref, turned):
    blocks = in_ref.shape[0]
    sequences, _, head = out_ref.shape
    rows = head // blocks
    later = jnp.zeros((sequences, head), F32)
    factors = [None] * blocks
    for b in reversed(range(blocks)):
        factors[b] = jnp.exp(later)
        later = later + in_ref[b, head : head + sequences, :]
    rest = jnp.zeros((head - blocks * sequences, head), F32)
    turned[...] = jnp.transpose(jnp.concatenate([*factors, rest], axis=0))
    mine = turned[pl.ds(pl.multiple_of(lax.axis_index(NEAR) * rows, rows), rows), :]
    for s in range(sequences):
        total = jnp.zeros((rows, head), F32)
        for b in range(blocks):
            column = mine[:, b * sequences + s : b * sequences + s + 1]
            total = total + in_ref[b, s * rows : (s + 1) * rows, :] * column
        out_ref[s, :rows, :] = total
        out_ref[s, rows:, :] = later


def far_kernel(in_ref, weight_ref, state_ref, part_ref, turned):
    blocks = in_ref.shape[0]
    rows, head = state_ref.shape
    s = lax.axis_index(HI)
    later = jnp.zeros((1, head), F32)
    factors = [None] * blocks
    for b in reversed(range(blocks)):
        factors[b] = jnp.exp(later)
        later = later + in_ref[b, pl.ds(rows + s, 1), :]
    weight = weight_ref[pl.ds(s, 1), :]
    rest = jnp.zeros((head - blocks - 1, head), F32)
    turned[...] = jnp.transpose(jnp.concatenate([*factors, weight, rest], axis=0))
    mine = turned[pl.ds(pl.multiple_of(lax.axis_index(NEAR) * rows, rows), rows), :]
    total = jnp.zeros((rows, head), F32)
    for b in range(blocks):
        total = total + in_ref[b, :rows, :] * mine[:, b : b + 1]
    state_ref[...] = total.astype(state_ref.dtype)
    part = jnp.sum(total * mine[:, blocks : blocks + 1], axis=0, keepdims=True)
    part_ref[...] = jnp.broadcast_to(part, part_ref.shape)


def token_kernel(
    token_ref, wq_ref, wf_ref, wv_ref, wg_ref, gap_ref, gain_ref, weight_ref, own_ref, gate_ref
):
    token = jnp.concatenate([token_ref[k] for k in range(token_ref.shape[0])], axis=1)
    query, forget, value, gate = (
        jnp.dot(token, ref[...], preferred_element_type=F32)
        for ref in (wq_ref, wf_ref, wv_ref, wg_ref)
    )
    loss = gap_ref[...] * jax.nn.sigmoid(-forget)
    weight_ref[...] = query * (1.0 - loss)
    own = jnp.sum(query * loss, axis=1, keepdims=True)
    own_ref[...] = own * value.astype(BF16).astype(F32)
    gate_ref[...] = gain_ref[...] * (gate * jax.nn.sigmoid(gate))


def read_kernel(part_ref, own_ref, gate_ref, out_ref):
    sequences, head = own_ref.shape
    parts = part_ref[...].reshape(sequences, part_ref.shape[0] // sequences, head)
    mixed = jnp.sum(parts, axis=1) + own_ref[...]
    scale = lax.rsqrt(jnp.mean(mixed * mixed, axis=1, keepdims=True) + EPSILON)
    out_ref[...] = (mixed * scale * gate_ref[...]).astype(out_ref.dtype)


def cost(flops, bytes_accessed):
    return pl.CostEstimate(flops=flops, bytes_accessed=bytes_accessed, transcendentals=0)


ANY = pl.BlockSpec(memory_space=pl.ANY)
VMEM = pl.BlockSpec(memory_space=pltpu.VMEM)


def per_device(
    prompt, keep_scale, new_token, w_query, w_forget, w_value, w_outgate, floor_gap, norm_gain
):
    sequences, positions, width = prompt.shape
    head = norm_gain.shape[0]
    near = lax.axis_size(NEAR)
    far = lax.axis_size(HI)
    rows = head // near
    gap = floor_gap.reshape(1, head)
    gain = norm_gain.reshape(1, head)
    shaped = jax.ShapeDtypeStruct

    tp = lax.axis_size(TP)
    token = lax.all_to_all(
        jnp.broadcast_to(new_token[None], (tp, *new_token.shape)), TP, 0, 0, tiled=True
    )
    states = pl.pallas_call(
        state_kernel,
        out_shape=shaped((near, head + sequences, head), F32),
        in_specs=[ANY, VMEM, VMEM, ANY, ANY],
        out_specs=VMEM,
        scratch_shapes=[
            pltpu.VMEM(prompt.shape, BF16),
            pltpu.VMEM((width, 2 * head), BF16),
            pltpu.SemaphoreType.DMA((sequences // 2,)),
            pltpu.SemaphoreType.DMA((2,)),
        ],
        cost_estimate=cost(600_000_000, 4_000_000),
        name="block_states",
    )(prompt, keep_scale, gap, w_forget, w_value)
    states = lax.all_to_all(states, NEAR, 0, 0, tiled=True)
    states = pl.pallas_call(
        near_kernel,
        out_shape=shaped((far, rows + sequences, head), F32),
        in_specs=[VMEM],
        out_specs=VMEM,
        scratch_shapes=[pltpu.VMEM((head, head), F32)],
        cost_estimate=cost(1_000_000, 600_000),
        name="near_states",
    )(states)
    small = shaped((sequences, head), F32)
    weight, own, gate = pl.pallas_call(
        token_kernel,
        out_shape=(small, small, small),
        in_specs=[VMEM] * 7,
        out_specs=(VMEM,) * 3,
        cost_estimate=cost(20_000_000, 2_200_000),
        name="token",
    )(token, w_query, w_forget, w_value, w_outgate, gap, gain)
    states = lax.all_to_all(states, HI, 0, 0, tiled=True)
    final, part = pl.pallas_call(
        far_kernel,
        out_shape=(shaped((rows, head), BF16), shaped((near * far, head), F32)),
        in_specs=[VMEM] * 2,
        out_specs=(VMEM,) * 2,
        scratch_shapes=[pltpu.VMEM((head, head), F32)],
        cost_estimate=cost(1_000_000, 200_000),
        name="far_states",
    )(states, weight)
    part = lax.all_to_all(part[:, None, :], SP, 0, 0, tiled=True)[:, 0, :]
    first_read = pl.pallas_call(
        read_kernel,
        out_shape=shaped((sequences, head), BF16),
        in_specs=[VMEM] * 3,
        out_specs=VMEM,
        cost_estimate=cost(100_000, 40_000),
        name="read",
    )(part, own, gate)
    return final[None], first_read


def solution(mesh):
    finer = Mesh(mesh.devices.reshape(8, 2, 4, mesh.shape["tp"]), (HI, LO, Y, TP))
    placed = (
        P(None, SP, None),
        P(None, SP),
        P(None, TP),
        P(None, TP),
        P(None, TP),
        P(None, TP),
        P(None, TP),
        P(TP),
        P(),
    )
    return jax.shard_map(
        per_device,
        mesh=finer,
        in_specs=placed,
        out_specs=(P(TP, SP, None), P(None, TP)),
        check_vma=False,
    )
```

time: 123 us -> 86.5 us (0.70)
  blocking collectives: 55.8 us -> 36.5 us
  Pallas kernels: 0 us -> 14.5 us
  matrix products: 11.7 us -> 0 us
  starting transfers between devices: 28.5 us -> 19 us
  waiting for transfers between devices: 20.1 us -> 14 us
  other arithmetic: 3.03 us -> 0 us
    psum x2 -> x0, blocking collectives: 55.8 us -> none  [by_axis(): return functools.reduce(lax.psum, axes, x)]
    all_to_all x0 -> x2, blocking collectives: none -> 36.5 us  [the longest x1 19.9 us: per_device(): part = lax.all_to_all(part[:, None, :], SP, 0, 0, tiled=True)[:, 0, :]]
    pallas_call x0 -> x5, Pallas kernels: none -> 14.5 us  [the longest x1 6.63 us: per_device(): pl.pallas_call(state_kernel, out_shape=shaped((near, head + sequences, he...]
    dot_general x8 -> x0, matrix products: 11.7 us -> none  [the longest x4 4.57 us: per_device(): jnp.dot(portion, weight, preferred_element_type=jnp.float32)]
    all_to_all x3 -> x2, starting transfers between devices: 28.5 us -> 19 us  [the longest x1 13.2 us: per_device(): states = lax.all_to_all(states, HI, 0, 0, tiled=True)]
    all_to_all x3 -> x2, waiting for transfers between devices: 20.1 us -> 14 us  [the longest x1 12 us: per_device(): states = lax.all_to_all(states, HI, 0, 0, tiled=True)]
    broadcast_in_dim x2 -> x1, local copies, waits for them, and re-layouts: 2.15 us -> 0.61 us  [per_device(): jnp.broadcast_to(new_token[None], (tp, *new_token.shape))]
    another operation x1 -> x0, other arithmetic: 1.31 us -> none  [per_device(): inside_log = lax.cumsum(log_forget, axis=1, reverse=True) - log_forget]
  transfers between devices with their start and end apart: 3 -> 2, of which waited for: 2 -> 2; matrix products, arithmetic and copies ran while one was open for 8% -> 0% of each run, Pallas kernels for 0% -> 5%
where the time goes in v1:
time: 86.5 us; the launch traced here: 85.9 us
  blocking collectives  36.5 us (42%)
  starting transfers between devices  19 us (22%)
  Pallas kernels  14.5 us (17%)
  waiting for transfers between devices  14 us (16%)
  local copies, waits for them, and re-layouts  1.25 us (1%)
    all_to_all x1, blocking collectives, per_device(): part = lax.all_to_all(part[:, None, :], SP, 0, 0, tiled=True)[:, 0, :]  19.9 us
    all_to_all x1, blocking collectives, per_device(): states = lax.all_to_all(states, NEAR, 0, 0, tiled=True)  16.6 us
    all_to_all x1, starting transfers between devices, per_device(): states = lax.all_to_all(states, HI, 0, 0, tiled=True)  13.2 us
    all_to_all x1, waiting for transfers between devices, per_device(): states = lax.all_to_all(states, HI, 0, 0, tiled=True)  12 us
    pallas_call x1, Pallas kernels, per_device(): pl.pallas_call(state_kernel, out_shape=shaped((near, head + sequences, he...  6.63 us
    all_to_all x1, starting transfers between devices, per_device(): lax.all_to_all(jnp.broadcast_to(new_token[None], (tp, *new_token.shape)),...  5.76 us
    pallas_call x1, Pallas kernels, per_device(): pl.pallas_call(token_kernel, out_shape=(small, small, small), in_specs=[V...  2.55 us
    pallas_call x1, Pallas kernels, per_device(): pl.pallas_call(near_kernel, out_shape=shaped((far, rows + sequences, head...  2.1 us
  transfers between devices with their start and end apart: 2, of which 2 were waited for; matrix products, arithmetic and copies ran while one was open for 0% of the time, Pallas kernels for 5%

profile of v1, /device:TPU:2, one launch (start us, length us, event | category | flops | bytes accessed | tf_op | source)
XLA Modules:
  0.0 85.9 jit_solution(3171374737491896247)
XLA Ops:
  0.6 0.0 copy-start.2
  0.6 6.6 %block_states.1 = f32[8,136,128]{2,1,0:T(8,128)} custom-call(bf16[8,64,2048]{2,1,0:T(8,128)(2,1)} %prompt_ref.1, f32[8,64]{1,0:T(8,128)} %keep_ref.1, f32[1,128]{1,0:T(1,128)} %bitcast.9, bf16[2048,128]{1,0:T(8,128)(2,1)} %wf_ref.3, bf16[2048,128]{1,0:T(8,128)(2,1)} %wv_ref.3), custom_call_target="tpu_custom_call" | custom-call | flops 600000000 | bytes 4000000 | tf_op jit(solution)/shard_map/block_states/pallas_call | solution.py:184
  7.3 16.6 %all_to_all.20.in_ref = f32[8,136,128]{2,1,0:T(8,128)} all-to-all(f32[8,136,128]{2,1,0:T(8,128)} %block_states.1), channel_id=1, replica_groups=mesh['sp_hi'=8,'sp_lo'=2,'sp_y'=4,'tp'=8] {'sp_lo','sp_y'}, dimensions={0} | all-to-all | bytes 1114112 | tf_op jit(solution)/shard_map/all_to_all | solution.py:198
  23.9 0.0 copy-done.2
  23.9 0.6 broadcast_in_dim.12
  24.5 5.8 %all-to-all-start.2 = ((bf16[8,8,256]{2,1,0:T(8,128)(2,1)}), bf16[8,8,256]{2,1,0:T(8,128)(2,1)S(1)}, u32[]{:S(2)}, u32[]{:S(2)}) async-start(bf16[8,8,256]{2,1,0:T(8,128)(2,1)} %broadcast_in_dim.12), calls=%async_computation.2 | async-start | bytes 65536 | tf_op jit(solution)/shard_map/all_to_all | solution.py:181
  30.3 2.1 %near_states.1 = f32[8,24,128]{2,1,0:T(8,128)} custom-call(f32[8,136,128]{2,1,0:T(8,128)} %all_to_all.20.in_ref), custom_call_target="tpu_custom_call" | custom-call | flops 1000000 | bytes 600000 | tf_op jit(solution)/shard_map/near_states/pallas_call | solution.py:199
  32.4 1.9 %all-to-all-done.2.token_ref = bf16[8,8,256]{2,1,0:T(8,128)(2,1)S(1)} async-done(((bf16[8,8,256]{2,1,0:T(8,128)(2,1)}), bf16[8,8,256]{2,1,0:T(8,128)(2,1)S(1)}, u32[]{:S(2)}, u32[]{:S(2)}) %all-to-all-start.2) | async-done | bytes 32800 | tf_op jit(solution)/shard_map/all_to_all | solution.py:181
  34.3 0.0 copy-start.1
  34.3 13.2 %all-to-all-start.1 = ((f32[8,24,128]{2,1,0:T(8,128)}), f32[8,24,128]{2,1,0:T(8,128)S(1)}, u32[]{:S(2)}, u32[]{:S(2)}) async-start(f32[8,24,128]{2,1,0:T(8,128)} %near_states.1), calls=%async_computation.1 | async-start | bytes 196608 | tf_op jit(solution)/shard_map/all_to_all | solution.py:217
  47.5 0.0 copy-done.1
  47.5 2.5 %token_.1 = (f32[8,128]{1,0:T(8,128)}, f32[8,128]{1,0:T(8,128)}, f32[8,128]{1,0:T(8,128)}) custom-call(bf16[8,8,256]{2,1,0:T(8,128)(2,1)} %copy-done.1, bf16[2048,128]{1,0:T(8,128)(2,1)} %wq_ref.1, bf16[2048,128]{1,0:T(8,128)(2,1)} %wf_ref.3, bf16[2048,128]{1,0:T(8,128)(2,1)} %wv_ref.3, bf16[2048,128]{1,0:T(8,128)(2,1)} %wg_ref.1, f32[1,128]{1,0:T(1,128)} %bitcast.10, ...), custom_call_target="tpu_custom_call" | custom-call | flops 20000000 | bytes 2200000 | tf_op jit(solution)/shard_map/token/pallas_call | solution.py:209
  50.1 12.0 %all-to-all-done.1.in_ref = f32[8,24,128]{2,1,0:T(8,128)S(1)} async-done(((f32[8,24,128]{2,1,0:T(8,128)}), f32[8,24,128]{2,1,0:T(8,128)S(1)}, u32[]{:S(2)}, u32[]{:S(2)}) %all-to-all-start.1) | async-done | bytes 98336 | tf_op jit(solution)/shard_map/all_to_all | solution.py:217
  62.1 0.0 copy-start
  62.1 0.6 copy-done
  62.8 1.7 %far_states.1 = (bf16[16,128]{1,0:T(8,128)(2,1)}, f32[64,128]{1,0:T(8,128)}) custom-call(f32[8,24,128]{2,1,0:T(8,128)} %copy-done, f32[8,128]{1,0:T(8,128)} %get-tuple-element.7.weight_ref), custom_call_target="tpu_custom_call" | custom-call | flops 1000000 | bytes 200000 | tf_op jit(solution)/shard_map/far_states/pallas_call | solution.py:218
  64.5 19.9 %all_to_all.21 = f32[64,1,128]{2,1,0:T(1,128)} all-to-all(f32[64,1,128]{2,1,0:T(1,128)} %bitcast.8), channel_id=1, replica_groups=mesh['sp_hi'=8,'sp_lo'=2,'sp_y'=4,'tp'=8] {'sp_hi','sp_lo','sp_y'}, dimensions={0} | all-to-all | bytes 65536 | tf_op jit(solution)/shard_map/all_to_all | solution.py:227
  84.4 1.4 %read.1 = bf16[8,128]{1,0:T(8,128)(2,1)} custom-call(f32[64,128]{1,0:T(8,128)} %bitcast.7, f32[8,128]{1,0:T(8,128)} %get-tuple-element.10.own_ref, f32[8,128]{1,0:T(8,128)} %get-tuple-element.11.gate_ref), custom_call_target="tpu_custom_call" | custom-call | flops 100000 | bytes 40000 | tf_op jit(solution)/shard_map/read/pallas_call | solution.py:228
Async XLA Ops:
  0.6 23.3 %copy-start.2 = (bf16[8,256]{1,0:T(8,128)(2,1)S(1)}, bf16[8,256]{1,0:T(8,128)(2,1)}, u32[]{:S(2)}) copy-start(bf16[8,256]{1,0:T(8,128)(2,1)} %param.11) | copy-start | bytes 12292
  24.5 9.8 %all-to-all-start.2 = ((bf16[8,8,256]{2,1,0:T(8,128)(2,1)}), bf16[8,8,256]{2,1,0:T(8,128)(2,1)S(1)}, u32[]{:S(2)}, u32[]{:S(2)}) async-start(bf16[8,8,256]{2,1,0:T(8,128)(2,1)} %broadcast_in_dim.12), calls=%async_computation.2 | async-start | bytes 65536 | tf_op jit(solution)/shard_map/all_to_all | solution.py:181
  34.3 13.2 %copy-start.1 = (bf16[8,8,256]{2,1,0:T(8,128)(2,1)}, bf16[8,8,256]{2,1,0:T(8,128)(2,1)S(1)}, u32[]{:S(2)}) copy-start(bf16[8,8,256]{2,1,0:T(8,128)(2,1)S(1)} %all-to-all-done.2.token_ref) | copy-start | bytes 98308
  34.3 27.8 %all-to-all-start.1 = ((f32[8,24,128]{2,1,0:T(8,128)}), f32[8,24,128]{2,1,0:T(8,128)S(1)}, u32[]{:S(2)}, u32[]{:S(2)}) async-start(f32[8,24,128]{2,1,0:T(8,128)} %near_states.1), calls=%async_computation.1 | async-start | bytes 196608 | tf_op jit(solution)/shard_map/all_to_all | solution.py:217
  62.1 0.6 copy-start

commit v2 on v1

--- a/solution.py
+++ b/solution.py
@@ -1,5 +1,3 @@
-import functools
-
 import jax
 import jax.numpy as jnp
 from jax import lax
@@ -8,6 +6,7 @@
 from jax.sharding import Mesh
 from jax.sharding import PartitionSpec as P
 
+
 HI, LO, Y, TP = "sp_hi", "sp_lo", "sp_y", "tp"
 SP = (HI, LO, Y)
 NEAR = (LO, Y)
@@ -23,7 +22,8 @@
 
 
 def state_kernel(
-    prompt_ref, keep_ref, gap_ref, wf_ref, wv_ref, out_ref, x_buf, w_buf, p_sem, w_sem
+    prompt_ref, keep_ref, gap_ref, wf_ref, wv_ref, out_ref,
+    x_buf, w_buf, keep_buf, gap_buf, both_buf, p_sem, w_sem, s_sem,
 ):
     sequences, positions, width = prompt_ref.shape
     head = gap_ref.shape[1]
@@ -40,17 +40,23 @@
         )
         for n in range(sequences // 2)
     ]
-    for copy in (*weights, *chunks):
+    smalls = [
+        pltpu.make_async_copy(keep_ref, keep_buf, s_sem.at[0]),
+        pltpu.make_async_copy(gap_ref, gap_buf, s_sem.at[1]),
+    ]
+    for copy in (*smalls, *weights, *chunks):
         copy.start()
-    keep = keep_ref[...]
-    filler = jnp.ones((sequences, head - positions), F32)
-    keep_columns = jnp.transpose(jnp.concatenate([keep, filler], axis=1))[:positions]
-    log_columns = jnp.log(keep_columns)
     row = lax.broadcasted_iota(jnp.int32, (pair, pair), 0)
     column = lax.broadcasted_iota(jnp.int32, (pair, pair), 1)
     later_mask = (column > row) & (column // positions == row // positions)
     later_mask = later_mask.astype(F32).astype(BF16)
-    gap = gap_ref[...]
+    for copy in smalls:
+        copy.wait()
+    keep = keep_buf[...]
+    filler = jnp.ones((sequences, head - positions), F32)
+    keep_columns = jnp.transpose(jnp.concatenate([keep, filler], axis=1))[:positions]
+    log_columns = jnp.log(keep_columns)
+    gap = gap_buf[...]
 
     def spread(columns, n):
         return jnp.concatenate(
@@ -66,7 +72,9 @@
     for n, copy in enumerate(chunks):
         copy.wait()
         x = x_buf[pl.ds(2 * n, 2)].reshape(pair, width)
-        both = jnp.dot(x, w_buf[...], preferred_element_type=F32)
+        both_buf[n] = jnp.dot(x, w_buf[...], preferred_element_type=F32)
+    for n in range(sequences // 2):
+        both = both_buf[n]
         values = both[:, head:].astype(BF16)
         loss = gap * jax.nn.sigmoid(-both[:, :head])
         keep_factor = spread(keep_columns, n)
@@ -134,10 +142,27 @@
     part_ref[...] = jnp.broadcast_to(part, part_ref.shape)
 
 
+def token_route(size, shift):
+    if shift == 1:
+        return [(i, i ^ 1) for i in range(size)]
+    return [(i, (i + shift) % size) for i in range(size)]
+
+
 def token_kernel(
-    token_ref, wq_ref, wf_ref, wv_ref, wg_ref, gap_ref, gain_ref, weight_ref, own_ref, gate_ref
+    own_part, part_1, part_2, part_4, wq_ref, wf_ref, wv_ref, wg_ref, gap_ref, gain_ref,
+    weight_ref, own_ref, gate_ref, token_buf,
 ):
-    token = jnp.concatenate([token_ref[k] for k in range(token_ref.shape[0])], axis=1)
+    size = lax.axis_size(TP)
+    me = lax.axis_index(TP)
+    width = own_part.shape[1]
+    parts = jnp.concatenate([own_part[...], part_1[...], part_2[...], part_4[...]], axis=1)
+    parity = lax.rem(me, 2)
+    for k in range(size):
+        side = parity if k % 2 == 0 else 1 - parity
+        owner = lax.rem((me - parity) + size - 2 * (k // 2), size) + side
+        start = pl.multiple_of(owner * width, width)
+        token_buf[:, pl.ds(start, width)] = parts[:, k * width : (k + 1) * width]
+    token = token_buf[...]
     query, forget, value, gate = (
         jnp.dot(token, ref[...], preferred_element_type=F32)
         for ref in (wq_ref, wf_ref, wv_ref, wg_ref)
@@ -161,11 +186,15 @@
     return pl.CostEstimate(flops=flops, bytes_accessed=bytes_accessed, transcendentals=0)
 
 
-ANY = pl.BlockSpec(memory_space=pl.ANY)
+def in_hbm(x):
+    return pltpu.with_memory_space_constraint(x, pltpu.HBM)
+
+
+HBM = pl.BlockSpec(memory_space=pltpu.HBM)
 VMEM = pl.BlockSpec(memory_space=pltpu.VMEM)
 
 
-def per_device(
+def device_step(
     prompt, keep_scale, new_token, w_query, w_forget, w_value, w_outgate, floor_gap, norm_gain
 ):
     sequences, positions, width = prompt.shape
@@ -177,24 +206,25 @@
     gain = norm_gain.reshape(1, head)
     shaped = jax.ShapeDtypeStruct
 
-    tp = lax.axis_size(TP)
-    token = lax.all_to_all(
-        jnp.broadcast_to(new_token[None], (tp, *new_token.shape)), TP, 0, 0, tiled=True
-    )
     states = pl.pallas_call(
         state_kernel,
         out_shape=shaped((near, head + sequences, head), F32),
-        in_specs=[ANY, VMEM, VMEM, ANY, ANY],
+        in_specs=[HBM] * 5,
         out_specs=VMEM,
         scratch_shapes=[
             pltpu.VMEM(prompt.shape, BF16),
             pltpu.VMEM((width, 2 * head), BF16),
+            pltpu.VMEM(keep_scale.shape, F32),
+            pltpu.VMEM(gap.shape, F32),
+            pltpu.VMEM((sequences // 2, 2 * positions, 2 * head), F32),
             pltpu.SemaphoreType.DMA((sequences // 2,)),
+            pltpu.SemaphoreType.DMA((2,)),
             pltpu.SemaphoreType.DMA((2,)),
         ],
         cost_estimate=cost(600_000_000, 4_000_000),
         name="block_states",
-    )(prompt, keep_scale, gap, w_forget, w_value)
+        compiler_params=pltpu.CompilerParams(vmem_limit_bytes=8 << 20),
+    )(*(in_hbm(x) for x in (prompt, keep_scale, gap, w_forget, w_value)))
     states = lax.all_to_all(states, NEAR, 0, 0, tiled=True)
     states = pl.pallas_call(
         near_kernel,
@@ -204,16 +234,24 @@
         scratch_shapes=[pltpu.VMEM((head, head), F32)],
         cost_estimate=cost(1_000_000, 600_000),
         name="near_states",
+        compiler_params=pltpu.CompilerParams(vmem_limit_bytes=4 << 20),
     )(states)
+    tp = lax.axis_size(TP)
+    pieces = [new_token]
+    for shift in (1, 2, 4):
+        sent = pieces[0] if shift == 1 else jnp.concatenate(pieces, axis=1)
+        pieces.append(lax.ppermute(sent, TP, token_route(tp, shift)))
     small = shaped((sequences, head), F32)
     weight, own, gate = pl.pallas_call(
         token_kernel,
         out_shape=(small, small, small),
-        in_specs=[VMEM] * 7,
+        in_specs=[VMEM] * 10,
         out_specs=(VMEM,) * 3,
+        scratch_shapes=[pltpu.VMEM((sequences, width), BF16)],
         cost_estimate=cost(20_000_000, 2_200_000),
         name="token",
-    )(token, w_query, w_forget, w_value, w_outgate, gap, gain)
+        compiler_params=pltpu.CompilerParams(vmem_limit_bytes=6 << 20),
+    )(*pieces, w_query, w_forget, w_value, w_outgate, gap, gain)
     states = lax.all_to_all(states, HI, 0, 0, tiled=True)
     final, part = pl.pallas_call(
         far_kernel,
@@ -223,6 +261,7 @@
         scratch_shapes=[pltpu.VMEM((head, head), F32)],
         cost_estimate=cost(1_000_000, 200_000),
         name="far_states",
+        compiler_params=pltpu.CompilerParams(vmem_limit_bytes=2 << 20),
     )(states, weight)
     part = lax.all_to_all(part[:, None, :], SP, 0, 0, tiled=True)[:, 0, :]
     first_read = pl.pallas_call(
@@ -232,6 +271,7 @@
         out_specs=VMEM,
         cost_estimate=cost(100_000, 40_000),
         name="read",
+        compiler_params=pltpu.CompilerParams(vmem_limit_bytes=1 << 20),
     )(part, own, gate)
     return final[None], first_read
 
@@ -250,7 +290,7 @@
         P(),
     )
     return jax.shard_map(
-        per_device,
+        device_step,
         mesh=finer,
         in_specs=placed,
         out_specs=(P(TP, SP, None), P(None, TP)),

time: 86.5 us -> 83 us (0.960)
  the two profiles are of different devices: /device:TPU:2 before, /device:TPU:8 now
where the time goes in v2:
time: 83 us; the launch traced here: 82.7 us
  blocking collectives  44 us (53%)
  starting transfers between devices  22.7 us (27%)
  waiting for transfers between devices  7.89 us (10%)
  Pallas kernels  7.24 us (9%)
    all_to_all x1, blocking collectives, device_step(): part = lax.all_to_all(part[:, None, :], SP, 0, 0, tiled=True)[:, 0, :]  28.2 us
    all_to_all x1, blocking collectives, device_step(): states = lax.all_to_all(states, NEAR, 0, 0, tiled=True)  15.8 us
    all_to_all x1, starting transfers between devices, device_step(): states = lax.all_to_all(states, HI, 0, 0, tiled=True)  13.7 us
    ppermute x3, starting transfers between devices, device_step(): pieces.append(lax.ppermute(sent, TP, token_route(tp, shift)))  9.02 us
    ppermute x3, waiting for transfers between devices, device_step(): pieces.append(lax.ppermute(sent, TP, token_route(tp, shift)))  7.89 us
    pallas_call x1, Pallas kernels, device_step(): pl.pallas_call(state_kernel, out_shape=shaped((near, head + sequences, he...  4.31 us
  transfers between devices with their start and end apart: 4, of which 3 were waited for; matrix products, arithmetic and copies ran while one was open for 0% of the time, Pallas kernels for 0%

profile of v2, /device:TPU:8, one launch (start us, length us, event | category | flops | bytes accessed | tf_op | source)
XLA Modules:
  0.0 82.7 jit_solution(3313157305810942178)
XLA Ops:
  0.6 0.0 copy-start.4
  0.6 0.0 copy-start
  0.7 0.0 copy-start.1
  0.7 0.0 copy-start.2
  0.7 0.0 copy-start.3
  0.7 0.0 copy-start.5
  0.7 0.0 copy-start.6
  0.7 4.3 %block_states.1 = f32[8,136,128]{2,1,0:T(8,128)S(1)} custom-call(bf16[8,64,2048]{2,1,0:T(8,128)(2,1)} %prompt_ref.1, f32[8,64]{1,0:T(8,128)} %keep_ref.1, f32[1,128]{1,0:T(1,128)} %bitcast.9, bf16[2048,128]{1,0:T(8,128)(2,1)} %wf_ref.3, bf16[2048,128]{1,0:T(8,128)(2,1)} %wv_ref.3), custom_call_target="tpu_custom_call" | custom-call | flops 600000000 | bytes 4000000 | tf_op jit(solution)/shard_map/block_states/pallas_call | solution.py:209
  5.0 15.8 %all_to_all.15.in_ref = f32[8,136,128]{2,1,0:T(8,128)S(1)} all-to-all(f32[8,136,128]{2,1,0:T(8,128)S(1)} %block_states.1), channel_id=1, replica_groups=mesh['sp_hi'=8,'sp_lo'=2,'sp_y'=4,'tp'=8] {'sp_lo','sp_y'}, dimensions={0} | all-to-all | bytes 1114112 | tf_op jit(solution)/shard_map/all_to_all | solution.py:228
  20.8 1.0 %near_states.1 = f32[8,24,128]{2,1,0:T(8,128)} custom-call(f32[8,136,128]{2,1,0:T(8,128)S(1)} %all_to_all.15.in_ref), custom_call_target="tpu_custom_call" | custom-call | flops 1000000 | bytes 600000 | tf_op jit(solution)/shard_map/near_states/pallas_call | solution.py:229
  21.8 13.7 %all-to-all-start.1 = ((f32[8,24,128]{2,1,0:T(8,128)}), f32[8,24,128]{2,1,0:T(8,128)S(1)}, u32[]{:S(2)}, u32[]{:S(2)}) async-start(f32[8,24,128]{2,1,0:T(8,128)} %near_states.1), calls=%async_computation.1 | async-start | bytes 196608 | tf_op jit(solution)/shard_map/all_to_all | solution.py:255
  35.5 0.0 copy-done.4
  35.5 1.9 %collective-permute-start = (bf16[8,256]{1,0:T(8,128)(2,1)S(1)}, bf16[8,256]{1,0:T(8,128)(2,1)S(1)}, u32[]{:S(2)}, u32[]{:S(2)}) collective-permute-start(bf16[8,256]{1,0:T(8,128)(2,1)S(1)} %copy-done.4), channel_id=1, source_target_pairs={{0,1},{1,0},{2,3},{3,2},{4,5},{5,4},{6,7},{7,6},{8,9},{9,8},{10,11... | collective-permute-start | bytes 12296 | tf_op jit(solution)/shard_map/ppermute | solution.py:243
  37.5 1.1 %collective-permute-done.part_1 = bf16[8,256]{1,0:T(8,128)(2,1)S(1)} collective-permute-done((bf16[8,256]{1,0:T(8,128)(2,1)S(1)}, bf16[8,256]{1,0:T(8,128)(2,1)S(1)}, u32[]{:S(2)}, u32[]{:S(2)}) %collective-permute-start) | collective-permute-done | bytes 4128 | tf_op jit(solution)/shard_map/ppermute | solution.py:243
  38.6 3.4 %collective-permute-start.1 = (bf16[8,512]{1,0:T(8,128)(2,1)S(1)}, bf16[8,512]{1,0:T(8,128)(2,1)S(1)}, u32[]{:S(2)}, u32[]{:S(2)}) collective-permute-start(bf16[8,512]{1,0:T(8,128)(2,1)S(1)} %pad_maximum_fusion.1), channel_id=1, source_target_pairs={{0,2},{1,3},{2,4},{3,5},{4,6},{5,7},{6,0},{7,1},{8,10},{9,11},{10,... | collective-permute-start | bytes 24584 | tf_op jit(solution)/shard_map/ppermute | solution.py:243
  42.0 3.3 %collective-permute-done.1.part_2 = bf16[8,512]{1,0:T(8,128)(2,1)S(1)} collective-permute-done((bf16[8,512]{1,0:T(8,128)(2,1)S(1)}, bf16[8,512]{1,0:T(8,128)(2,1)S(1)}, u32[]{:S(2)}, u32[]{:S(2)}) %collective-permute-start.1) | collective-permute-done | bytes 8224 | tf_op jit(solution)/shard_map/ppermute | solution.py:243
  45.4 3.7 %collective-permute-start.2 = (bf16[8,1024]{1,0:T(8,128)(2,1)S(1)}, bf16[8,1024]{1,0:T(8,128)(2,1)S(1)}, u32[]{:S(2)}, u32[]{:S(2)}) collective-permute-start(bf16[8,1024]{1,0:T(8,128)(2,1)S(1)} %pad_maximum_fusion), channel_id=1, source_target_pairs={{0,4},{1,5},{2,6},{3,7},{4,0},{5,1},{6,2},{7,3},{8,12},{9,13},{10,... | collective-permute-start | bytes 49160 | tf_op jit(solution)/shard_map/ppermute | solution.py:243
  49.1 3.4 %collective-permute-done.2.part_4 = bf16[8,1024]{1,0:T(8,128)(2,1)S(1)} collective-permute-done((bf16[8,1024]{1,0:T(8,128)(2,1)S(1)}, bf16[8,1024]{1,0:T(8,128)(2,1)S(1)}, u32[]{:S(2)}, u32[]{:S(2)}) %collective-permute-start.2) | collective-permute-done | bytes 16416 | tf_op jit(solution)/shard_map/ppermute | solution.py:243
  52.5 0.0 copy-done
  52.5 0.0 copy-done.1
  52.5 0.0 copy-done.2
  52.5 0.0 copy-done.3
  52.5 0.0 copy-done.5
  52.5 0.0 copy-done.6
  52.5 0.4 token_.1
  52.9 0.0 all-to-all-done.1.in_ref
  52.9 0.8 %far_states.1 = (bf16[16,128]{1,0:T(8,128)(2,1)}, f32[64,128]{1,0:T(8,128)S(1)}) custom-call(f32[8,24,128]{2,1,0:T(8,128)S(1)} %all-to-all-done.1.in_ref, f32[8,128]{1,0:T(8,128)S(1)} %get-tuple-element.7.weight_ref), custom_call_target="tpu_custom_call" | custom-call | flops 1000000 | bytes 200000 | tf_op jit(solution)/shard_map/far_states/pallas_call | solution.py:256
  53.8 28.2 %all_to_all.16 = f32[64,1,128]{2,1,0:T(1,128)S(1)} all-to-all(f32[64,1,128]{2,1,0:T(1,128)S(1)} %bitcast.8), channel_id=1, replica_groups=mesh['sp_hi'=8,'sp_lo'=2,'sp_y'=4,'tp'=8] {'sp_hi','sp_lo','sp_y'}, dimensions={0} | all-to-all | bytes 65536 | tf_op jit(solution)/shard_map/all_to_all | solution.py:266
  82.0 0.7 read.1
  (2 shorter events, 0.0 us)
Async XLA Ops:
  0.6 34.9 %copy-start.4 = (bf16[8,256]{1,0:T(8,128)(2,1)S(1)}, bf16[8,256]{1,0:T(8,128)(2,1)}, u32[]{:S(2)}) copy-start(bf16[8,256]{1,0:T(8,128)(2,1)} %own_part.1) | copy-start | bytes 12292
  0.6 51.8 %copy-start = (bf16[2048,128]{1,0:T(8,128)(2,1)S(1)}, bf16[2048,128]{1,0:T(8,128)(2,1)}, u32[]{:S(2)}) copy-start(bf16[2048,128]{1,0:T(8,128)(2,1)} %wf_ref.3) | copy-start | bytes 1572868
  0.7 51.8 %copy-start.1 = (bf16[2048,128]{1,0:T(8,128)(2,1)S(1)}, bf16[2048,128]{1,0:T(8,128)(2,1)}, u32[]{:S(2)}) copy-start(bf16[2048,128]{1,0:T(8,128)(2,1)} %wv_ref.3) | copy-start | bytes 1572868
  0.7 51.8 %copy-start.2 = (bf16[2048,128]{1,0:T(8,128)(2,1)S(1)}, bf16[2048,128]{1,0:T(8,128)(2,1)}, u32[]{:S(2)}) copy-start(bf16[2048,128]{1,0:T(8,128)(2,1)} %wq_ref.1) | copy-start | bytes 1572868
  0.7 51.8 %copy-start.3 = (bf16[2048,128]{1,0:T(8,128)(2,1)S(1)}, bf16[2048,128]{1,0:T(8,128)(2,1)}, u32[]{:S(2)}) copy-start(bf16[2048,128]{1,0:T(8,128)(2,1)} %wg_ref.1) | copy-start | bytes 1572868
  0.7 51.8 %copy-start.5 = (f32[128]{0:T(128)S(1)}, f32[128]{0:T(128)}, u32[]{:S(2)}) copy-start(f32[128]{0:T(128)} %param.16) | copy-start | bytes 1540
  0.7 51.8 %copy-start.6 = (f32[128]{0:T(128)S(1)}, f32[128]{0:T(128)}, u32[]{:S(2)}) copy-start(f32[128]{0:T(128)} %param.17) | copy-start | bytes 1540
  21.8 31.1 %all-to-all-start.1 = ((f32[8,24,128]{2,1,0:T(8,128)}), f32[8,24,128]{2,1,0:T(8,128)S(1)}, u32[]{:S(2)}, u32[]{:S(2)}) async-start(f32[8,24,128]{2,1,0:T(8,128)} %near_states.1), calls=%async_computation.1 | async-start | bytes 196608 | tf_op jit(solution)/shard_map/all_to_all | solution.py:255
  35.5 3.1 %collective-permute-start = (bf16[8,256]{1,0:T(8,128)(2,1)S(1)}, bf16[8,256]{1,0:T(8,128)(2,1)S(1)}, u32[]{:S(2)}, u32[]{:S(2)}) collective-permute-start(bf16[8,256]{1,0:T(8,128)(2,1)S(1)} %copy-done.4), channel_id=1, source_target_pairs={{0,1},{1,0},{2,3},{3,2},{4,5},{5,4},{6,7},{7,6},{8,9},{9,8},{10,11... | collective-permute-start | bytes 12296 | tf_op jit(solution)/shard_map/ppermute | solution.py:243
  38.6 6.7 %collective-permute-start.1 = (bf16[8,512]{1,0:T(8,128)(2,1)S(1)}, bf16[8,512]{1,0:T(8,128)(2,1)S(1)}, u32[]{:S(2)}, u32[]{:S(2)}) collective-permute-start(bf16[8,512]{1,0:T(8,128)(2,1)S(1)} %pad_maximum_fusion.1), channel_id=1, source_target_pairs={{0,2},{1,3},{2,4},{3,5},{4,6},{5,7},{6,0},{7,1},{8,10},{9,11},{10,... | collective-permute-start | bytes 24584 | tf_op jit(solution)/shard_map/ppermute | solution.py:243
  45.4 7.1 %collective-permute-start.2 = (bf16[8,1024]{1,0:T(8,128)(2,1)S(1)}, bf16[8,1024]{1,0:T(8,128)(2,1)S(1)}, u32[]{:S(2)}, u32[]{:S(2)}) collective-permute-start(bf16[8,1024]{1,0:T(8,128)(2,1)S(1)} %pad_maximum_fusion), channel_id=1, source_target_pairs={{0,4},{1,5},{2,6},{3,7},{4,0},{5,1},{6,2},{7,3},{8,12},{9,13},{10,... | collective-permute-start | bytes 49160 | tf_op jit(solution)/shard_map/ppermute | solution.py:243

commit v3 on v2

--- a/solution.py
+++ b/solution.py
@@ -1,3 +1,5 @@
+import functools
+
 import jax
 import jax.numpy as jnp
 from jax import lax
@@ -11,6 +13,20 @@
 SP = (HI, LO, Y)
 NEAR = (LO, Y)
 EPSILON = 1e-06
+
+
+def ring_from_middle(size):
+    return [(size // 2 + k) % size for k in range(size)]
+
+
+def near_order(low, y):
+    return [l * y + m for l in range(low) for m in ring_from_middle(y)]
+
+
+def read_order(far, near):
+    return [h * len(near) + j for h in ring_from_middle(far) for j in near]
+
+
 F32, BF16 = jnp.float32, jnp.bfloat16
 
 
@@ -22,7 +38,7 @@
 
 
 def state_kernel(
-    prompt_ref, keep_ref, gap_ref, wf_ref, wv_ref, out_ref,
+    order, prompt_ref, keep_ref, gap_ref, wf_ref, wv_ref, out_ref,
     x_buf, w_buf, keep_buf, gap_buf, both_buf, p_sem, w_sem, s_sem,
 ):
     sequences, positions, width = prompt_ref.shape
@@ -95,12 +111,12 @@
             )
             first = k * positions
             total = later[first : first + 1] + log_forget[first : first + 1]
-            for j in range(peers):
-                out_ref[j, s * rows : (s + 1) * rows, :] = state[j * rows : (j + 1) * rows]
-                out_ref[j, head + s : head + s + 1, :] = total
-
-
-def near_kernel(in_ref, out_ref, turned):
+            for r, j in enumerate(order):
+                out_ref[r, s * rows : (s + 1) * rows, :] = state[j * rows : (j + 1) * rows]
+                out_ref[r, head + s : head + s + 1, :] = total
+
+
+def near_kernel(order, far_ranks, in_ref, out_ref, turned):
     blocks = in_ref.shape[0]
     sequences, _, head = out_ref.shape
     rows = head // blocks
@@ -108,7 +124,7 @@
     factors = [None] * blocks
     for b in reversed(range(blocks)):
         factors[b] = jnp.exp(later)
-        later = later + in_ref[b, head : head + sequences, :]
+        later = later + in_ref[order.index(b), head : head + sequences, :]
     rest = jnp.zeros((head - blocks * sequences, head), F32)
     turned[...] = jnp.transpose(jnp.concatenate([*factors, rest], axis=0))
     mine = turned[pl.ds(pl.multiple_of(lax.axis_index(NEAR) * rows, rows), rows), :]
@@ -116,12 +132,12 @@
         total = jnp.zeros((rows, head), F32)
         for b in range(blocks):
             column = mine[:, b * sequences + s : b * sequences + s + 1]
-            total = total + in_ref[b, s * rows : (s + 1) * rows, :] * column
-        out_ref[s, :rows, :] = total
-        out_ref[s, rows:, :] = later
-
-
-def far_kernel(in_ref, weight_ref, state_ref, part_ref, turned):
+            total = total + in_ref[order.index(b), s * rows : (s + 1) * rows, :] * column
+        out_ref[far_ranks.index(s), :rows, :] = total
+        out_ref[far_ranks.index(s), rows:, :] = later
+
+
+def far_kernel(order, in_ref, weight_ref, state_ref, part_ref, turned):
     blocks = in_ref.shape[0]
     rows, head = state_ref.shape
     s = lax.axis_index(HI)
@@ -129,14 +145,14 @@
     factors = [None] * blocks
     for b in reversed(range(blocks)):
         factors[b] = jnp.exp(later)
-        later = later + in_ref[b, pl.ds(rows + s, 1), :]
+        later = later + in_ref[order.index(b), pl.ds(rows + s, 1), :]
     weight = weight_ref[pl.ds(s, 1), :]
     rest = jnp.zeros((head - blocks - 1, head), F32)
     turned[...] = jnp.transpose(jnp.concatenate([*factors, weight, rest], axis=0))
     mine = turned[pl.ds(pl.multiple_of(lax.axis_index(NEAR) * rows, rows), rows), :]
     total = jnp.zeros((rows, head), F32)
     for b in range(blocks):
-        total = total + in_ref[b, :rows, :] * mine[:, b : b + 1]
+        total = total + in_ref[order.index(b), :rows, :] * mine[:, b : b + 1]
     state_ref[...] = total.astype(state_ref.dtype)
     part = jnp.sum(total * mine[:, blocks : blocks + 1], axis=0, keepdims=True)
     part_ref[...] = jnp.broadcast_to(part, part_ref.shape)
@@ -149,19 +165,17 @@
 
 
 def token_kernel(
-    own_part, part_1, part_2, part_4, wq_ref, wf_ref, wv_ref, wg_ref, gap_ref, gain_ref,
+    same_ref, swapped_ref, wq_ref, wf_ref, wv_ref, wg_ref, gap_ref, gain_ref,
     weight_ref, own_ref, gate_ref, token_buf,
 ):
     size = lax.axis_size(TP)
     me = lax.axis_index(TP)
-    width = own_part.shape[1]
-    parts = jnp.concatenate([own_part[...], part_1[...], part_2[...], part_4[...]], axis=1)
-    parity = lax.rem(me, 2)
-    for k in range(size):
-        side = parity if k % 2 == 0 else 1 - parity
-        owner = lax.rem((me - parity) + size - 2 * (k // 2), size) + side
-        start = pl.multiple_of(owner * width, width)
-        token_buf[:, pl.ds(start, width)] = parts[:, k * width : (k + 1) * width]
+    width = token_buf.shape[1] // size
+    for ref, core in ((same_ref, lax.rem(me, 2)), (swapped_ref, 1 - lax.rem(me, 2))):
+        for k in range(size // 2):
+            owner = lax.rem(me - lax.rem(me, 2) + size - 2 * k, size) + core
+            start = pl.multiple_of(owner * width, width)
+            token_buf[:, pl.ds(start, width)] = ref[:, k * width : (k + 1) * width]
     token = token_buf[...]
     query, forget, value, gate = (
         jnp.dot(token, ref[...], preferred_element_type=F32)
@@ -177,13 +191,19 @@
 def read_kernel(part_ref, own_ref, gate_ref, out_ref):
     sequences, head = own_ref.shape
     parts = part_ref[...].reshape(sequences, part_ref.shape[0] // sequences, head)
-    mixed = jnp.sum(parts, axis=1) + own_ref[...]
+    mixed = jnp.sum(parts, axis=1)
+    half = sequences // 2
+    mixed = jnp.concatenate([mixed[half:], mixed[:half]], axis=0) + own_ref[...]
     scale = lax.rsqrt(jnp.mean(mixed * mixed, axis=1, keepdims=True) + EPSILON)
     out_ref[...] = (mixed * scale * gate_ref[...]).astype(out_ref.dtype)
 
 
 def cost(flops, bytes_accessed):
     return pl.CostEstimate(flops=flops, bytes_accessed=bytes_accessed, transcendentals=0)
+
+
+def exchanged(x, axes, ranks):
+    return lax.all_to_all(x, axes, 0, 0, tiled=True, axis_index_groups=[ranks])
 
 
 def in_hbm(x):
@@ -202,12 +222,15 @@
     near = lax.axis_size(NEAR)
     far = lax.axis_size(HI)
     rows = head // near
+    near_ranks = near_order(lax.axis_size(LO), lax.axis_size(Y))
+    far_ranks = ring_from_middle(far)
+    read_ranks = read_order(far, near_ranks)
     gap = floor_gap.reshape(1, head)
     gain = norm_gain.reshape(1, head)
     shaped = jax.ShapeDtypeStruct
 
     states = pl.pallas_call(
-        state_kernel,
+        functools.partial(state_kernel, near_ranks),
         out_shape=shaped((near, head + sequences, head), F32),
         in_specs=[HBM] * 5,
         out_specs=VMEM,
@@ -225,9 +248,9 @@
         name="block_states",
         compiler_params=pltpu.CompilerParams(vmem_limit_bytes=8 << 20),
     )(*(in_hbm(x) for x in (prompt, keep_scale, gap, w_forget, w_value)))
-    states = lax.all_to_all(states, NEAR, 0, 0, tiled=True)
+    states = exchanged(states, NEAR, near_ranks)
     states = pl.pallas_call(
-        near_kernel,
+        functools.partial(near_kernel, near_ranks, far_ranks),
         out_shape=shaped((far, rows + sequences, head), F32),
         in_specs=[VMEM],
         out_specs=VMEM,
@@ -237,24 +260,26 @@
         compiler_params=pltpu.CompilerParams(vmem_limit_bytes=4 << 20),
     )(states)
     tp = lax.axis_size(TP)
-    pieces = [new_token]
-    for shift in (1, 2, 4):
-        sent = pieces[0] if shift == 1 else jnp.concatenate(pieces, axis=1)
-        pieces.append(lax.ppermute(sent, TP, token_route(tp, shift)))
+    received = {}
+    for shift in (2, 4, 6):
+        received[shift] = lax.ppermute(new_token, TP, token_route(tp, shift))
+    pieces = lax.optimization_barrier(jnp.concatenate([new_token, received[2]], axis=1))
+    pieces = jnp.concatenate([pieces, received[4], received[6]], axis=1)
+    swapped = lax.ppermute(pieces, TP, token_route(tp, 1))
     small = shaped((sequences, head), F32)
     weight, own, gate = pl.pallas_call(
         token_kernel,
         out_shape=(small, small, small),
-        in_specs=[VMEM] * 10,
+        in_specs=[VMEM] * 8,
         out_specs=(VMEM,) * 3,
         scratch_shapes=[pltpu.VMEM((sequences, width), BF16)],
         cost_estimate=cost(20_000_000, 2_200_000),
         name="token",
         compiler_params=pltpu.CompilerParams(vmem_limit_bytes=6 << 20),
-    )(*pieces, w_query, w_forget, w_value, w_outgate, gap, gain)
-    states = lax.all_to_all(states, HI, 0, 0, tiled=True)
+    )(pieces, swapped, w_query, w_forget, w_value, w_outgate, gap, gain)
+    states = exchanged(states, HI, far_ranks)
     final, part = pl.pallas_call(
-        far_kernel,
+        functools.partial(far_kernel, far_ranks),
         out_shape=(shaped((rows, head), BF16), shaped((near * far, head), F32)),
         in_specs=[VMEM] * 2,
         out_specs=(VMEM,) * 2,
@@ -263,7 +288,7 @@
         name="far_states",
         compiler_params=pltpu.CompilerParams(vmem_limit_bytes=2 << 20),
     )(states, weight)
-    part = lax.all_to_all(part[:, None, :], SP, 0, 0, tiled=True)[:, 0, :]
+    part = exchanged(part[:, None, :], SP, read_ranks)[:, 0, :]
     first_read = pl.pallas_call(
         read_kernel,
         out_shape=shaped((sequences, head), BF16),

time: 83 us -> 75.7 us (0.912)
  blocking collectives: 44 us -> 34 us
  starting transfers between devices: 22.7 us -> 28.7 us
  waiting for transfers between devices: 7.89 us -> 4.4 us
    all_to_all x2, blocking collectives: 44 us -> 34 us  [exchanged(): return lax.all_to_all(x, axes, 0, 0, tiled=True, axis_index_groups=[ranks])]
    ppermute x3 -> x4, starting transfers between devices: 9.02 us -> 12.7 us  [the longest x3 10.8 us: device_step(): received[shift] = lax.ppermute(new_token, TP, token_route(tp, shift))]
    ppermute x3 -> x4, waiting for transfers between devices: 7.89 us -> 4.4 us  [the longest x3 3.25 us: device_step(): received[shift] = lax.ppermute(new_token, TP, token_route(tp, shift))]
    all_to_all x1, starting transfers between devices: 13.7 us -> 16.1 us  [exchanged(): return lax.all_to_all(x, axes, 0, 0, tiled=True, axis_index_groups=[ranks])]
  transfers between devices with their start and end apart: 4 -> 5, of which waited for: 3 -> 2; matrix products, arithmetic and copies ran while one was open for 0% -> 0% of each run, Pallas kernels for 0% -> 1%
where the time goes in v3:
time: 75.7 us; the launch traced here: 75.2 us
  blocking collectives  34 us (45%)
  starting transfers between devices  28.7 us (38%)
  Pallas kernels  7.25 us (10%)
  waiting for transfers between devices  4.4 us (6%)
  between operations  0.8 us (1%)
    all_to_all x2, blocking collectives, exchanged(): return lax.all_to_all(x, axes, 0, 0, tiled=True, axis_index_groups=[ranks])  34 us
    all_to_all x1, starting transfers between devices, exchanged(): return lax.all_to_all(x, axes, 0, 0, tiled=True, axis_index_groups=[ranks])  16.1 us
    ppermute x3, starting transfers between devices, device_step(): received[shift] = lax.ppermute(new_token, TP, token_route(tp, shift))  10.8 us
    pallas_call x1, Pallas kernels, device_step(): pl.pallas_call(functools.partial(state_kernel, near_ranks), out_shape=sha...  4.31 us
    ppermute x3, waiting for transfers between devices, device_step(): received[shift] = lax.ppermute(new_token, TP, token_route(tp, shift))  3.25 us
    ppermute x1, starting transfers between devices, device_step(): swapped = lax.ppermute(pieces, TP, token_route(tp, 1))  1.91 us
  transfers between devices with their start and end apart: 5, of which 2 were waited for; matrix products, arithmetic and copies ran while one was open for 0% of the time, Pallas kernels for 1%

profile of v3, /device:TPU:8, one launch (start us, length us, event | category | flops | bytes accessed | tf_op | source)
XLA Modules:
  0.0 75.2 jit_solution(3140261790587492432)
XLA Ops:
  0.6 0.0 copy-start.6
  0.6 0.0 copy-start
  0.7 0.0 copy-start.1
  0.7 0.0 copy-start.2
  0.7 0.0 copy-start.3
  0.7 0.0 copy-start.4
  0.7 0.0 copy-start.5
  0.7 4.3 %block_states.1 = f32[8,136,128]{2,1,0:T(8,128)S(1)} custom-call(bf16[8,64,2048]{2,1,0:T(8,128)(2,1)} %prompt_ref.1, f32[8,64]{1,0:T(8,128)} %keep_ref.1, f32[1,128]{1,0:T(1,128)} %bitcast.9, bf16[2048,128]{1,0:T(8,128)(2,1)} %wf_ref.3, bf16[2048,128]{1,0:T(8,128)(2,1)} %wv_ref.3), custom_call_target="tpu_custom_call" | custom-call | flops 600000000 | bytes 4000000 | tf_op jit(solution)/shard_map/block_states/pallas_call | solution.py:232
  5.0 16.0 %all_to_all.15.in_ref = f32[8,136,128]{2,1,0:T(8,128)S(1)} all-to-all(f32[8,136,128]{2,1,0:T(8,128)S(1)} %block_states.1), channel_id=1, replica_groups={{16,24,0,8,48,56,32,40},{17,25,1,9,49,57,33,41},{18,26,2,10,50,58,34,42..., dimensions={0} | all-to-all | bytes 1114112 | tf_op jit(solution)/shard_map/all_to_all | solution.py:206
  21.0 1.0 %near_states.1 = f32[8,24,128]{2,1,0:T(8,128)} custom-call(f32[8,136,128]{2,1,0:T(8,128)S(1)} %all_to_all.15.in_ref), custom_call_target="tpu_custom_call" | custom-call | flops 1000000 | bytes 600000 | tf_op jit(solution)/shard_map/near_states/pallas_call | solution.py:252
  22.0 16.1 %all-to-all-start.1 = ((f32[8,24,128]{2,1,0:T(8,128)}), f32[8,24,128]{2,1,0:T(8,128)S(1)}, u32[]{:S(2)}, u32[]{:S(2)}) async-start(f32[8,24,128]{2,1,0:T(8,128)} %near_states.1), calls=%async_computation.1 | async-start | bytes 196608 | tf_op jit(solution)/shard_map/all_to_all | solution.py:206
  38.1 0.0 copy-done.6
  38.1 3.4 %collective-permute-start = (bf16[8,256]{1,0:T(8,128)(2,1)S(1)}, bf16[8,256]{1,0:T(8,128)(2,1)S(1)}, u32[]{:S(2)}, u32[]{:S(2)}) collective-permute-start(bf16[8,256]{1,0:T(8,128)(2,1)S(1)} %copy-done.6), channel_id=1, source_target_pairs={{0,2},{1,3},{2,4},{3,5},{4,6},{5,7},{6,0},{7,1},{8,10},{9,11},{10,... | collective-permute-start | bytes 12296 | tf_op jit(solution)/shard_map/ppermute | solution.py:265
  41.5 3.7 %collective-permute-start.2 = (bf16[8,256]{1,0:T(8,128)(2,1)S(1)}, bf16[8,256]{1,0:T(8,128)(2,1)S(1)}, u32[]{:S(2)}, u32[]{:S(2)}) collective-permute-start(bf16[8,256]{1,0:T(8,128)(2,1)S(1)} %copy-done.6), channel_id=1, source_target_pairs={{0,6},{1,7},{2,0},{3,1},{4,2},{5,3},{6,4},{7,5},{8,14},{9,15},{10,... | collective-permute-start | bytes 12296 | tf_op jit(solution)/shard_map/ppermute | solution.py:265
  45.2 3.7 %collective-permute-start.1 = (bf16[8,256]{1,0:T(8,128)(2,1)S(1)}, bf16[8,256]{1,0:T(8,128)(2,1)S(1)}, u32[]{:S(2)}, u32[]{:S(2)}) collective-permute-start(bf16[8,256]{1,0:T(8,128)(2,1)S(1)} %copy-done.6), channel_id=1, source_target_pairs={{0,4},{1,5},{2,6},{3,7},{4,0},{5,1},{6,2},{7,3},{8,12},{9,13},{10,... | collective-permute-start | bytes 12296 | tf_op jit(solution)/shard_map/ppermute | solution.py:265
  48.9 0.0 collective-permute-done
  48.9 0.0 collective-permute-done.2
  48.9 3.2 %collective-permute-done.1 = bf16[8,256]{1,0:T(8,128)(2,1)S(1)} collective-permute-done((bf16[8,256]{1,0:T(8,128)(2,1)S(1)}, bf16[8,256]{1,0:T(8,128)(2,1)S(1)}, u32[]{:S(2)}, u32[]{:S(2)}) %collective-permute-start.1) | collective-permute-done | bytes 4128 | tf_op jit(solution)/shard_map/ppermute | solution.py:265
  52.2 1.9 %collective-permute-start.3 = (bf16[8,1024]{1,0:T(8,128)(2,1)S(1)}, bf16[8,1024]{1,0:T(8,128)(2,1)S(1)}, u32[]{:S(2)}, u32[]{:S(2)}) collective-permute-start(bf16[8,1024]{1,0:T(8,128)(2,1)S(1)} %pad_maximum_fusion.same_ref), channel_id=1, source_target_pairs={{0,1},{1,0},{2,3},{3,2},{4,5},{5,4},{6,7},{7,6},{8,9},{9,8},{10,11... | collective-permute-start | bytes 49160 | tf_op jit(solution)/shard_map/ppermute | solution.py:268
  54.1 1.1 %collective-permute-done.3.swapped_ref = bf16[8,1024]{1,0:T(8,128)(2,1)S(1)} collective-permute-done((bf16[8,1024]{1,0:T(8,128)(2,1)S(1)}, bf16[8,1024]{1,0:T(8,128)(2,1)S(1)}, u32[]{:S(2)}, u32[]{:S(2)}) %collective-permute-start.3) | collective-permute-done | bytes 16416 | tf_op jit(solution)/shard_map/ppermute | solution.py:268
  55.2 0.0 copy-done
  55.2 0.0 copy-done.1
  55.2 0.0 copy-done.2
  55.2 0.0 copy-done.3
  55.3 0.0 copy-done.4
  55.3 0.0 copy-done.5
  55.3 0.4 token_.1
  55.7 0.0 all-to-all-done.1.in_ref
  55.7 0.8 %far_states.1 = (bf16[16,128]{1,0:T(8,128)(2,1)}, f32[64,128]{1,0:T(8,128)S(1)}) custom-call(f32[8,24,128]{2,1,0:T(8,128)S(1)} %all-to-all-done.1.in_ref, f32[8,128]{1,0:T(8,128)S(1)} %get-tuple-element.7.weight_ref), custom_call_target="tpu_custom_call" | custom-call | flops 1000000 | bytes 200000 | tf_op jit(solution)/shard_map/far_states/pallas_call | solution.py:281
  56.5 18.1 %all_to_all.16 = f32[64,1,128]{2,1,0:T(1,128)S(1)} all-to-all(f32[64,1,128]{2,1,0:T(1,128)S(1)} %bitcast.8), channel_id=1, replica_groups={{272,280,256,264,304,312,288,296,336,344,320,328,368,376,352,360,400,40..., dimensions={0} | all-to-all | bytes 65536 | tf_op jit(solution)/shard_map/all_to_all | solution.py:206
  74.6 0.7 read.1
  (2 shorter events, 0.0 us)
Async XLA Ops:
  0.6 37.5 %copy-start.6 = (bf16[8,256]{1,0:T(8,128)(2,1)S(1)}, bf16[8,256]{1,0:T(8,128)(2,1)}, u32[]{:S(2)}) copy-start(bf16[8,256]{1,0:T(8,128)(2,1)} %param.11) | copy-start | bytes 12292
  0.6 54.6 %copy-start = (bf16[2048,128]{1,0:T(8,128)(2,1)S(1)}, bf16[2048,128]{1,0:T(8,128)(2,1)}, u32[]{:S(2)}) copy-start(bf16[2048,128]{1,0:T(8,128)(2,1)} %wf_ref.3) | copy-start | bytes 1572868
  0.7 54.6 %copy-start.1 = (bf16[2048,128]{1,0:T(8,128)(2,1)S(1)}, bf16[2048,128]{1,0:T(8,128)(2,1)}, u32[]{:S(2)}) copy-start(bf16[2048,128]{1,0:T(8,128)(2,1)} %wv_ref.3) | copy-start | bytes 1572868
  0.7 54.6 %copy-start.2 = (bf16[2048,128]{1,0:T(8,128)(2,1)S(1)}, bf16[2048,128]{1,0:T(8,128)(2,1)}, u32[]{:S(2)}) copy-start(bf16[2048,128]{1,0:T(8,128)(2,1)} %wq_ref.1) | copy-start | bytes 1572868
  0.7 54.6 %copy-start.3 = (bf16[2048,128]{1,0:T(8,128)(2,1)S(1)}, bf16[2048,128]{1,0:T(8,128)(2,1)}, u32[]{:S(2)}) copy-start(bf16[2048,128]{1,0:T(8,128)(2,1)} %wg_ref.1) | copy-start | bytes 1572868
  0.7 54.6 %copy-start.4 = (f32[128]{0:T(128)S(1)}, f32[128]{0:T(128)}, u32[]{:S(2)}) copy-start(f32[128]{0:T(128)} %param.16) | copy-start | bytes 1540
  0.7 54.6 %copy-start.5 = (f32[128]{0:T(128)S(1)}, f32[128]{0:T(128)}, u32[]{:S(2)}) copy-start(f32[128]{0:T(128)} %param.17) | copy-start | bytes 1540
  22.0 33.6 %all-to-all-start.1 = ((f32[8,24,128]{2,1,0:T(8,128)}), f32[8,24,128]{2,1,0:T(8,128)S(1)}, u32[]{:S(2)}, u32[]{:S(2)}) async-start(f32[8,24,128]{2,1,0:T(8,128)} %near_states.1), calls=%async_computation.1 | async-start | bytes 196608 | tf_op jit(solution)/shard_map/all_to_all | solution.py:206
  38.1 10.8 %collective-permute-start = (bf16[8,256]{1,0:T(8,128)(2,1)S(1)}, bf16[8,256]{1,0:T(8,128)(2,1)S(1)}, u32[]{:S(2)}, u32[]{:S(2)}) collective-permute-start(bf16[8,256]{1,0:T(8,128)(2,1)S(1)} %copy-done.6), channel_id=1, source_target_pairs={{0,2},{1,3},{2,4},{3,5},{4,6},{5,7},{6,0},{7,1},{8,10},{9,11},{10,... | collective-permute-start | bytes 12296 | tf_op jit(solution)/shard_map/ppermute | solution.py:265
  41.5 7.4 %collective-permute-start.2 = (bf16[8,256]{1,0:T(8,128)(2,1)S(1)}, bf16[8,256]{1,0:T(8,128)(2,1)S(1)}, u32[]{:S(2)}, u32[]{:S(2)}) collective-permute-start(bf16[8,256]{1,0:T(8,128)(2,1)S(1)} %copy-done.6), channel_id=1, source_target_pairs={{0,6},{1,7},{2,0},{3,1},{4,2},{5,3},{6,4},{7,5},{8,14},{9,15},{10,... | collective-permute-start | bytes 12296 | tf_op jit(solution)/shard_map/ppermute | solution.py:265
  45.2 7.0 %collective-permute-start.1 = (bf16[8,256]{1,0:T(8,128)(2,1)S(1)}, bf16[8,256]{1,0:T(8,128)(2,1)S(1)}, u32[]{:S(2)}, u32[]{:S(2)}) collective-permute-start(bf16[8,256]{1,0:T(8,128)(2,1)S(1)} %copy-done.6), channel_id=1, source_target_pairs={{0,4},{1,5},{2,6},{3,7},{4,0},{5,1},{6,2},{7,3},{8,12},{9,13},{10,... | collective-permute-start | bytes 12296 | tf_op jit(solution)/shard_map/ppermute | solution.py:265
  52.2 3.1 %collective-permute-start.3 = (bf16[8,1024]{1,0:T(8,128)(2,1)S(1)}, bf16[8,1024]{1,0:T(8,128)(2,1)S(1)}, u32[]{:S(2)}, u32[]{:S(2)}) collective-permute-start(bf16[8,1024]{1,0:T(8,128)(2,1)S(1)} %pad_maximum_fusion.same_ref), channel_id=1, source_target_pairs={{0,1},{1,0},{2,3},{3,2},{4,5},{5,4},{6,7},{7,6},{8,9},{9,8},{10,11... | collective-permute-start | bytes 49160 | tf_op jit(solution)/shard_map/ppermute | solution.py:268

commit v4 on v1

v4 whole, which is shorter than its diff:
```python
import functools

import jax
import jax.numpy as jnp
from jax import lax
from jax.experimental import pallas as pl
from jax.experimental.pallas import tpu as pltpu
from jax.sharding import Mesh
from jax.sharding import PartitionSpec as P

HI, LO, Y, TP = "sp_hi", "sp_lo", "sp_y", "tp"
SP = (HI, LO, Y)
NEAR = (LO, Y)
EPSILON = 1e-06


def ring_from_middle(size):
    return [(size // 2 + k) % size for k in range(size)]


def near_order(low, y):
    return [l * y + m for l in range(low) for m in ring_from_middle(y)]


def read_order(far, near):
    return [h * len(near) + j for h in ring_from_middle(far) for j in near]

F32, BF16 = jnp.float32, jnp.bfloat16


def in_two(x):
    high = x.astype(BF16)
    return high, (x - high.astype(F32)).astype(BF16)


def opening_kernel(out_ref):
    out_ref[...] = jnp.zeros_like(out_ref)


def state_kernel(
    order, opening_ref, prompt_ref, keep_ref, gap_ref, wf_ref, wv_ref, out_ref, total_ref, both_buf
):
    del opening_ref
    sequences, positions, width = prompt_ref.shape
    head = gap_ref.shape[1]
    peers = out_ref.shape[0]
    rows = head // peers
    pair = 2 * positions
    row = lax.broadcasted_iota(jnp.int32, (pair, pair), 0)
    column = lax.broadcasted_iota(jnp.int32, (pair, pair), 1)
    later_mask = (column > row) & (column // positions == row // positions)
    later_mask = later_mask.astype(F32).astype(BF16)
    filler = jnp.ones((sequences, head - positions), F32)
    keep_columns = jnp.transpose(jnp.concatenate([keep_ref[...], filler], axis=1))[:positions]
    log_columns = jnp.log(keep_columns)
    gap = gap_ref[...]

    def spread(columns, n):
        return jnp.concatenate(
            [
                jnp.broadcast_to(columns[:, s : s + 1], (positions, head))
                for s in (2 * n, 2 * n + 1)
            ],
            axis=0,
        )

    x = prompt_ref[...].reshape(sequences * positions, width)
    weights = jnp.concatenate([wf_ref[...], wv_ref[...]], axis=1)
    both_buf[...] = jnp.dot(x, weights, preferred_element_type=F32)
    for n in range(sequences // 2):
        both = both_buf[n * pair : (n + 1) * pair]
        values = both[:, head:].astype(BF16)
        loss = gap * jax.nn.sigmoid(-both[:, :head])
        keep_factor = spread(keep_columns, n)
        log_forget = spread(log_columns, n) + jnp.log1p(-loss)
        gate = (1.0 - keep_factor) + keep_factor * loss
        later = sum(
            jnp.dot(later_mask, part, preferred_element_type=F32)
            for part in in_two(log_forget)
        )
        gated = in_two(gate * jnp.exp(later))
        for k in range(2):
            s = 2 * n + k
            span = slice(k * positions, (k + 1) * positions)
            left = jnp.concatenate([part[span] for part in gated], axis=0)
            right = jnp.concatenate([values[span]] * 2, axis=0)
            state = lax.dot_general(
                left, right, (((0,), (0,)), ((), ())), preferred_element_type=F32
            )
            first = k * positions
            total_ref[s : s + 1, :] = later[first : first + 1] + log_forget[first : first + 1]
            for r, j in enumerate(order):
                out_ref[r, s * rows : (s + 1) * rows, :] = state[j * rows : (j + 1) * rows]


def token_route(near, tp):
    return [
        (j * tp + (i + j) % tp, j * tp + i) for j in range(near) for i in range(tp)
    ]


def chunk_of_lane(shape, rows):
    return lax.broadcasted_iota(jnp.int32, shape, len(shape) - 1) // rows


def token_kernel(
    order, token_ref, totals_ref, wq_ref, wf_ref, wv_ref, wg_ref, states_ref, out_ref,
    tile_buf, sem,
):
    del states_ref
    size = lax.axis_size(TP)
    width = token_ref.shape[1]
    peers, tile_rows, head = tile_buf.shape
    rows = head // peers
    block = lax.rem(lax.axis_index(TP) + lax.axis_index(NEAR), size)
    span = pl.ds(pl.multiple_of(block * width, width), width)
    token = token_ref[...]
    picked = lax.broadcasted_iota(jnp.int32, (token.shape[0], 1), 0) == lax.axis_index(HI)
    tile = []
    for ref in (wq_ref, wf_ref, wv_ref, wg_ref):
        part = jnp.dot(token, ref[span, :], preferred_element_type=F32)
        part = jnp.sum(jnp.where(picked, part, 0.0), axis=0, keepdims=True)
        tile += [part, pltpu.roll(part, rows, 1)]
    tile = jnp.concatenate(tile, axis=0)
    totals = totals_ref[...]
    chunk = chunk_of_lane(tile.shape, rows)
    for r, j in enumerate(order):
        tile_buf[r] = jnp.where(chunk == j, totals, tile)
    last = pl.ds(out_ref.shape[1] - tile_rows, tile_rows)
    copy = pltpu.make_async_copy(tile_buf, out_ref.at[:, last], sem)
    copy.start()
    copy.wait()


def near_kernel(order, far_ranks, in_ref, gap_ref, gain_ref, out_ref, token_ref, turned):
    blocks = in_ref.shape[0]
    sequences, _, head = out_ref.shape
    rows = head // blocks
    later = jnp.zeros((sequences, head), F32)
    factors = [None] * blocks
    for b in reversed(range(blocks)):
        factors[b] = jnp.exp(later)
        later = later + in_ref[order.index(b), head : head + sequences, :]
    rest = jnp.zeros((head - blocks * sequences, head), F32)
    turned[...] = jnp.transpose(jnp.concatenate([*factors, rest], axis=0))
    mine = turned[pl.ds(pl.multiple_of(lax.axis_index(NEAR) * rows, rows), rows), :]
    for s in range(sequences):
        total = jnp.zeros((rows, head), F32)
        for b in range(blocks):
            column = mine[:, b * sequences + s : b * sequences + s + 1]
            total = total + in_ref[order.index(b), s * rows : (s + 1) * rows, :] * column
        out_ref[far_ranks.index(s), :rows, :] = total
        out_ref[far_ranks.index(s), rows : rows + 1, :] = later[s : s + 1]
    tiles = sum(in_ref[b, head:, :] for b in range(blocks))
    own_chunk = chunk_of_lane((1, head), rows) == lax.axis_index(NEAR)
    query, forget, value, gate = (
        jnp.where(
            own_chunk,
            pltpu.roll(tiles[2 * k + 1 : 2 * k + 2], head - rows, 1),
            tiles[2 * k : 2 * k + 1],
        )
        for k in range(4)
    )
    loss = gap_ref[...] * jax.nn.sigmoid(-forget)
    own = jnp.sum(query * loss, axis=1, keepdims=True) * value.astype(BF16).astype(F32)
    own = jnp.where(lax.axis_index(NEAR) == 0, own, 0.0)
    token_ref[...] = jnp.concatenate(
        [query * (1.0 - loss), own, jnp.zeros((sequences - 2, head), F32)], axis=0
    )
    gate = gain_ref[...] * (gate * jax.nn.sigmoid(gate))
    spare = jnp.zeros((sequences - 2, head), F32)
    for r in range(sequences):
        out_ref[r, rows + 1 :, :] = jnp.concatenate([gate, spare], axis=0)


def far_kernel(order, in_ref, token_ref, state_ref, part_ref, gate_ref, turned):
    blocks = in_ref.shape[0]
    rows, head = state_ref.shape
    later = jnp.zeros((1, head), F32)
    factors = [None] * blocks
    for b in reversed(range(blocks)):
        factors[b] = jnp.exp(later)
        later = later + in_ref[order.index(b), rows : rows + 1, :]
        gate_ref[b : b + 1, :] = in_ref[order.index(b), rows + 1 : rows + 2, :]
    weight, own = (token_ref[k : k + 1, :] for k in range(2))
    rest = jnp.zeros((head - blocks - 1, head), F32)
    turned[...] = jnp.transpose(jnp.concatenate([*factors, weight, rest], axis=0))
    mine = turned[pl.ds(pl.multiple_of(lax.axis_index(NEAR) * rows, rows), rows), :]
    total = jnp.zeros((rows, head), F32)
    for b in range(blocks):
        total = total + in_ref[order.index(b), :rows, :] * mine[:, b : b + 1]
    state_ref[...] = total.astype(state_ref.dtype)
    part = jnp.sum(total * mine[:, blocks : blocks + 1], axis=0, keepdims=True) + own
    part_ref[...] = jnp.broadcast_to(part, part_ref.shape)


def read_kernel(part_ref, gate_ref, out_ref):
    sequences, head = out_ref.shape
    parts = part_ref[...].reshape(sequences, part_ref.shape[0] // sequences, head)
    mixed = jnp.sum(parts, axis=1)
    half = sequences // 2
    mixed = jnp.concatenate([mixed[half:], mixed[:half]], axis=0)
    scale = lax.rsqrt(jnp.mean(mixed * mixed, axis=1, keepdims=True) + EPSILON)
    out_ref[...] = (mixed * scale * gate_ref[...]).astype(out_ref.dtype)


def cost(flops, bytes_accessed):
    return pl.CostEstimate(flops=flops, bytes_accessed=bytes_accessed, transcendentals=0)


def exchanged(x, axes, ranks):
    return lax.all_to_all(x, axes, 0, 0, tiled=True, axis_index_groups=[ranks])


ANY = pl.BlockSpec(memory_space=pl.ANY)
VMEM = pl.BlockSpec(memory_space=pltpu.VMEM)


def per_device(
    prompt, keep_scale, new_token, w_query, w_forget, w_value, w_outgate, floor_gap, norm_gain
):
    sequences, positions, width = prompt.shape
    head = norm_gain.shape[0]
    near = lax.axis_size(NEAR)
    far = lax.axis_size(HI)
    rows = head // near
    near_ranks = near_order(lax.axis_size(LO), lax.axis_size(Y))
    far_ranks = ring_from_middle(far)
    read_ranks = read_order(far, near_ranks)
    gap = floor_gap.reshape(1, head)
    gain = norm_gain.reshape(1, head)
    shaped = jax.ShapeDtypeStruct

    head_start = pl.pallas_call(
        opening_kernel,
        out_shape=shaped((8, head), F32),
        out_specs=VMEM,
        cost_estimate=cost(20_000_000_000, 40_000_000),
        name="opening",
        compiler_params=pltpu.CompilerParams(vmem_limit_bytes=1 << 20),
    )()
    new_token, head_start = lax.optimization_barrier((new_token, head_start))
    token = lax.ppermute(new_token, (*NEAR, TP), token_route(near, lax.axis_size(TP)))
    states, totals = pl.pallas_call(
        functools.partial(state_kernel, near_ranks),
        out_shape=(
            shaped((near, head + sequences, head), F32),
            shaped((sequences, head), F32),
        ),
        in_specs=[VMEM] * 6,
        out_specs=(VMEM,) * 2,
        scratch_shapes=[pltpu.VMEM((sequences * positions, 2 * head), F32)],
        cost_estimate=cost(600_000_000, 4_000_000),
        name="block_states",
        compiler_params=pltpu.CompilerParams(vmem_limit_bytes=8 << 20),
    )(head_start, prompt, keep_scale, gap, w_forget, w_value)
    states = pl.pallas_call(
        functools.partial(token_kernel, near_ranks),
        out_shape=shaped(states.shape, F32),
        in_specs=[VMEM] * 6 + [ANY],
        out_specs=ANY,
        scratch_shapes=[pltpu.VMEM((near, sequences, head), F32), pltpu.SemaphoreType.DMA],
        input_output_aliases={6: 0},
        cost_estimate=cost(2_000_000, 300_000),
        name="token",
        compiler_params=pltpu.CompilerParams(vmem_limit_bytes=6 << 20),
    )(token, totals, w_query, w_forget, w_value, w_outgate, states)
    states = exchanged(states, NEAR, near_ranks)
    states, token_rows = pl.pallas_call(
        functools.partial(near_kernel, near_ranks, far_ranks),
        out_shape=(
            shaped((far, rows + sequences, head), F32),
            shaped((sequences, head), F32),
        ),
        in_specs=[VMEM] * 3,
        out_specs=(VMEM,) * 2,
        scratch_shapes=[pltpu.VMEM((head, head), F32)],
        cost_estimate=cost(1_000_000, 600_000),
        name="near_states",
        compiler_params=pltpu.CompilerParams(vmem_limit_bytes=4 << 20),
    )(states, gap, gain)
    states = exchanged(states, HI, far_ranks)
    final, part, gate = pl.pallas_call(
        functools.partial(far_kernel, far_ranks),
        out_shape=(
            shaped((rows, head), BF16),
            shaped((near * far, head), F32),
            shaped((sequences, head), F32),
        ),
        in_specs=[VMEM] * 2,
        out_specs=(VMEM,) * 3,
        scratch_shapes=[pltpu.VMEM((head, head), F32)],
        cost_estimate=cost(1_000_000, 200_000),
        name="far_states",
        compiler_params=pltpu.CompilerParams(vmem_limit_bytes=2 << 20),
    )(states, token_rows)
    part = exchanged(part[:, None, :], SP, read_ranks)[:, 0, :]
    first_read = pl.pallas_call(
        read_kernel,
        out_shape=shaped((sequences, head), BF16),
        in_specs=[VMEM] * 2,
        out_specs=VMEM,
        cost_estimate=cost(100_000, 40_000),
        name="read",
        compiler_params=pltpu.CompilerParams(vmem_limit_bytes=1 << 20),
    )(part, gate)
    return final[None], first_read


def solution(mesh):
    finer = Mesh(mesh.devices.reshape(8, 2, 4, mesh.shape["tp"]), (HI, LO, Y, TP))
    placed = (
        P(None, SP, None),
        P(None, SP),
        P(None, TP),
        P(None, TP),
        P(None, TP),
        P(None, TP),
        P(None, TP),
        P(TP),
        P(),
    )
    return jax.shard_map(
        per_device,
        mesh=finer,
        in_specs=placed,
        out_specs=(P(TP, SP, None), P(None, TP)),
        check_vma=False,
    )
```

time: 86.5 us -> 64.6 us (0.75)
  the two profiles are of different devices: /device:TPU:2 before, /device:TPU:8 now
where the time goes in v4:
time: 64.6 us; the launch traced here: 64.3 us
  blocking collectives  54.6 us (85%)
  starting transfers between devices  4.23 us (7%)
  Pallas kernels  4.04 us (6%)
  between operations  0.78 us (1%)
  local copies, waits for them, and re-layouts  0.65 us (1%)
    all_to_all x3, blocking collectives, exchanged(): return lax.all_to_all(x, axes, 0, 0, tiled=True, axis_index_groups=[ranks])  54.6 us
    ppermute x1, starting transfers between devices, per_device(): lax.ppermute(new_token, (*NEAR, TP), token_route(near, lax.axis_size(TP)))  4.23 us
    pallas_call x1, Pallas kernels, per_device(): pl.pallas_call(functools.partial(state_kernel, near_ranks), out_shape=(sh...  1.83 us
  transfers between devices with their start and end apart: 1, of which 0 were waited for; matrix products, arithmetic and copies ran while one was open for 0% of the time, Pallas kernels for 3%

profile of v4, /device:TPU:8, one launch (start us, length us, event | category | flops | bytes accessed | tf_op | source)
XLA Modules:
  0.0 64.3 jit_solution(10522943043240793268)
XLA Ops:
  0.6 0.0 copy-start.8
  0.6 0.0 copy-start.2
  0.7 0.0 copy-start.1
  0.7 0.0 copy-start.6
  0.7 0.0 copy-start.5
  0.7 0.0 copy-start
  0.7 0.6 copy-done.8
  1.3 0.0 copy-start.3
  1.3 0.0 copy-start.4
  1.3 4.2 %collective-permute-start = (bf16[8,256]{1,0:T(8,128)(2,1)S(1)}, bf16[8,256]{1,0:T(8,128)(2,1)S(1)}, u32[]{:S(2)}, u32[]{:S(2)}) collective-permute-start(bf16[8,256]{1,0:T(8,128)(2,1)S(1)} %copy-done.8), channel_id=1, source_target_pairs={{0,0},{1,1},{2,2},{3,3},{4,4},{5,5},{6,6},{7,7},{9,8},{10,9},{11,1... | collective-permute-start | bytes 12296 | tf_op jit(solution)/shard_map/ppermute | solution.py:243
  5.6 0.0 copy-done.2
  5.6 0.0 copy-done.1
  5.6 0.0 copy-done.6
  5.6 0.0 copy-done.5
  5.6 0.0 copy-done
  5.6 1.8 %block_states.1 = (f32[8,136,128]{2,1,0:T(8,128)S(1)}, f32[8,128]{1,0:T(8,128)S(1)}) custom-call(f32[8,128]{1,0:T(8,128)S(1)} %opening.1.opening_ref, bf16[8,64,2048]{2,1,0:T(8,128)(2,1)S(1)} %copy-done, f32[8,64]{1,0:T(8,128)S(1)} %copy-done.5, f32[1,128]{1,0:T(1,128)S(1)} %bitcast.9, bf16[2048,128]{1,0:T(8,128)(2,1)S(1)} %copy-done.1, ...), custom_call_target="tpu_custom_call" | custom-call | flops 600000000 | bytes 4000000 | tf_op jit(solution)/shard_map/block_states/pallas_call | solution.py:244
  7.4 0.0 collective-permute-done.token_ref
  7.5 0.0 copy-done.3
  7.5 0.0 copy-done.4
  7.5 0.0 copy-start.7
  7.5 0.3 token_.1
  7.8 14.8 %all_to_all.15.in_ref = f32[8,136,128]{2,1,0:T(8,128)S(1)} all-to-all(f32[8,136,128]{2,1,0:T(8,128)S(1)} %token_.1), channel_id=1, replica_groups={{16,24,0,8,48,56,32,40},{17,25,1,9,49,57,33,41},{18,26,2,10,50,58,34,42..., dimensions={0} | all-to-all | bytes 1114112 | tf_op jit(solution)/shard_map/all_to_all | solution.py:212
  22.6 0.0 copy-done.7
  22.6 0.4 near_states.1
  23.0 21.5 %all_to_all.16.in_ref = f32[8,24,128]{2,1,0:T(8,128)S(1)} all-to-all(f32[8,24,128]{2,1,0:T(8,128)S(1)} %get-tuple-element.15), channel_id=1, replica_groups={{256,320,384,448,0,64,128,192},{257,321,385,449,1,65,129,193},{258,322,..., dimensions={0} | all-to-all | bytes 196608 | tf_op jit(solution)/shard_map/all_to_all | solution.py:212
  44.5 0.8 %far_states.1 = (bf16[16,128]{1,0:T(8,128)(2,1)}, f32[64,128]{1,0:T(8,128)S(1)}, f32[8,128]{1,0:T(8,128)S(1)}) custom-call(f32[8,24,128]{2,1,0:T(8,128)S(1)} %all_to_all.16.in_ref, f32[8,128]{1,0:T(8,128)S(1)} %get-tuple-element.16.token_ref), custom_call_target="tpu_custom_call" | custom-call | flops 1000000 | bytes 200000 | tf_op jit(solution)/shard_map/far_states/pallas_call | solution.py:283
  45.3 18.3 %all_to_all.17 = f32[64,1,128]{2,1,0:T(1,128)S(1)} all-to-all(f32[64,1,128]{2,1,0:T(1,128)S(1)} %bitcast.8), channel_id=1, replica_groups={{272,280,256,264,304,312,288,296,336,344,320,328,368,376,352,360,400,40..., dimensions={0} | all-to-all | bytes 65536 | tf_op jit(solution)/shard_map/all_to_all | solution.py:212
  63.7 0.7 %read.1 = bf16[8,128]{1,0:T(8,128)(2,1)} custom-call(f32[64,128]{1,0:T(8,128)S(1)} %bitcast.7, f32[8,128]{1,0:T(8,128)S(1)} %get-tuple-element.19.gate_ref), custom_call_target="tpu_custom_call" | custom-call | flops 100000 | bytes 40000 | tf_op jit(solution)/shard_map/read/pallas_call | solution.py:298
  (1 shorter events, 0.0 us)
Async XLA Ops:
  0.6 0.7 %copy-start.8 = (bf16[8,256]{1,0:T(8,128)(2,1)S(1)}, bf16[8,256]{1,0:T(8,128)(2,1)}, u32[]{:S(2)}) copy-start(bf16[8,256]{1,0:T(8,128)(2,1)} %param.11) | copy-start | bytes 12292
  0.6 4.9 %copy-start.2 = (bf16[2048,128]{1,0:T(8,128)(2,1)S(1)}, bf16[2048,128]{1,0:T(8,128)(2,1)}, u32[]{:S(2)}) copy-start(bf16[2048,128]{1,0:T(8,128)(2,1)} %wv_ref.3) | copy-start | bytes 1572868
  0.7 4.9 %copy-start.1 = (bf16[2048,128]{1,0:T(8,128)(2,1)S(1)}, bf16[2048,128]{1,0:T(8,128)(2,1)}, u32[]{:S(2)}) copy-start(bf16[2048,128]{1,0:T(8,128)(2,1)} %wf_ref.3) | copy-start | bytes 1572868
  0.7 4.9 %copy-start.6 = (f32[128]{0:T(128)S(1)}, f32[128]{0:T(128)}, u32[]{:S(2)}) copy-start(f32[128]{0:T(128)} %param.16) | copy-start | bytes 1540
  0.7 4.9 %copy-start.5 = (f32[8,64]{1,0:T(8,128)S(1)}, f32[8,64]{1,0:T(8,128)}, u32[]{:S(2)}) copy-start(f32[8,64]{1,0:T(8,128)} %keep_ref.1) | copy-start | bytes 6148
  0.7 4.9 %copy-start = (bf16[8,64,2048]{2,1,0:T(8,128)(2,1)S(1)}, bf16[8,64,2048]{2,1,0:T(8,128)(2,1)}, u32[]{:S(2)}) copy-start(bf16[8,64,2048]{2,1,0:T(8,128)(2,1)} %prompt_ref.1) | copy-start | bytes 6291460
  1.3 6.1 %copy-start.3 = (bf16[2048,128]{1,0:T(8,128)(2,1)S(1)}, bf16[2048,128]{1,0:T(8,128)(2,1)}, u32[]{:S(2)}) copy-start(bf16[2048,128]{1,0:T(8,128)(2,1)} %wq_ref.1) | copy-start | bytes 1572868
  1.3 6.1 %copy-start.4 = (bf16[2048,128]{1,0:T(8,128)(2,1)S(1)}, bf16[2048,128]{1,0:T(8,128)(2,1)}, u32[]{:S(2)}) copy-start(bf16[2048,128]{1,0:T(8,128)(2,1)} %wg_ref.1) | copy-start | bytes 1572868
  1.3 6.1 %collective-permute-start = (bf16[8,256]{1,0:T(8,128)(2,1)S(1)}, bf16[8,256]{1,0:T(8,128)(2,1)S(1)}, u32[]{:S(2)}, u32[]{:S(2)}) collective-permute-start(bf16[8,256]{1,0:T(8,128)(2,1)S(1)} %copy-done.8), channel_id=1, source_target_pairs={{0,0},{1,1},{2,2},{3,3},{4,4},{5,5},{6,6},{7,7},{9,8},{10,9},{11,1... | collective-permute-start | bytes 12296 | tf_op jit(solution)/shard_map/ppermute | solution.py:243
  7.5 15.1 %copy-start.7 = (f32[128]{0:T(128)S(1)}, f32[128]{0:T(128)}, u32[]{:S(2)}) copy-start(f32[128]{0:T(128)} %param.17) | copy-start | bytes 1540

commit v5 on v4

v5 whole, which is shorter than its diff:
```python
import functools

import jax
import jax.numpy as jnp
from jax import lax
from jax.experimental import pallas as pl
from jax.experimental.pallas import tpu as pltpu
from jax.sharding import Mesh
from jax.sharding import PartitionSpec as P

HI, LO, Y, TP = "sp_hi", "sp_lo", "sp_y", "tp"
SP = (HI, LO, Y)
NEAR = (LO, Y)
EPSILON = 1e-06


FAR_ORDER, READ_ORDER, Y_ORDER = (4, 0, 7, 1, 6, 2, 5, 3), (4, 0, 7, 1, 6, 2, 5, 3), (2, 3, 0, 1)


F32, BF16 = jnp.float32, jnp.bfloat16


def near_order(low):
    return [l * len(Y_ORDER) + m for l in range(low) for m in Y_ORDER]


def read_order(near):
    return [h * len(near) + j for h in READ_ORDER for j in near]


def in_two(x):
    high = x.astype(BF16)
    return high, (x - high.astype(F32)).astype(BF16)


def opening_kernel(out_ref):
    out_ref[...] = jnp.zeros_like(out_ref)


def state_kernel(
    order, opening_ref, prompt_ref, keep_ref, gap_ref, wf_ref, wv_ref, out_ref, both_buf
):
    del opening_ref
    sequences, positions, width = prompt_ref.shape
    head = gap_ref.shape[1]
    peers = out_ref.shape[0]
    rows = head // peers
    pair = 2 * positions
    row = lax.broadcasted_iota(jnp.int32, (pair, pair), 0)
    column = lax.broadcasted_iota(jnp.int32, (pair, pair), 1)
    later_mask = (column > row) & (column // positions == row // positions)
    later_mask = later_mask.astype(F32).astype(BF16)
    filler = jnp.ones((sequences, head - positions), F32)
    keep_columns = jnp.transpose(jnp.concatenate([keep_ref[...], filler], axis=1))[:positions]
    log_columns = jnp.log(keep_columns)
    gap = gap_ref[...]

    def spread(columns, n):
        return jnp.concatenate(
            [
                jnp.broadcast_to(columns[:, s : s + 1], (positions, head))
                for s in (2 * n, 2 * n + 1)
            ],
            axis=0,
        )

    x = prompt_ref[...].reshape(sequences * positions, width)
    weights = jnp.concatenate([wf_ref[...], wv_ref[...]], axis=1)
    both_buf[...] = jnp.dot(x, weights, preferred_element_type=F32)
    for n in range(sequences // 2):
        both = both_buf[n * pair : (n + 1) * pair]
        values = both[:, head:].astype(BF16)
        loss = gap * jax.nn.sigmoid(-both[:, :head])
        keep_factor = spread(keep_columns, n)
        log_forget = spread(log_columns, n) + jnp.log1p(-loss)
        gate = (1.0 - keep_factor) + keep_factor * loss
        later = sum(
            jnp.dot(later_mask, part, preferred_element_type=F32)
            for part in in_two(log_forget)
        )
        gated = in_two(gate * jnp.exp(later))
        for k in range(2):
            s = 2 * n + k
            span = slice(k * positions, (k + 1) * positions)
            left = jnp.concatenate([part[span] for part in gated], axis=0)
            right = jnp.concatenate([values[span]] * 2, axis=0)
            state = lax.dot_general(
                left, right, (((0,), (0,)), ((), ())), preferred_element_type=F32
            )
            first = k * positions
            total = later[first : first + 1] + log_forget[first : first + 1]
            for r, j in enumerate(order):
                out_ref[r, s * rows : (s + 1) * rows, :] = state[j * rows : (j + 1) * rows]
                out_ref[r, head + s : head + s + 1, :] = total


def token_route(far, tp):
    return [(h * tp + (i + h) % tp, h * tp + i) for h in range(far) for i in range(tp)]


def near_kernel(
    order, far_ranks, in_ref, token_ref, wq_ref, wf_ref, wv_ref, wg_ref, out_ref, turned
):
    blocks = in_ref.shape[0]
    sequences, _, head = out_ref.shape
    rows = head // blocks
    width = token_ref.shape[1]
    block = lax.rem(lax.axis_index(TP) + lax.axis_index(HI), lax.axis_size(TP))
    span = pl.ds(pl.multiple_of(block * width, width), width)
    token = token_ref[...]
    parts = [
        jnp.dot(token, ref[span, :], preferred_element_type=F32)
        for ref in (wq_ref, wf_ref, wv_ref, wg_ref)
    ]
    later = jnp.zeros((sequences, head), F32)
    factors = [None] * blocks
    for b in reversed(range(blocks)):
        factors[b] = jnp.exp(later)
        later = later + in_ref[order.index(b), head : head + sequences, :]
    rest = jnp.zeros((head - blocks * sequences, head), F32)
    turned[...] = jnp.transpose(jnp.concatenate([*factors, rest], axis=0))
    mine = turned[pl.ds(pl.multiple_of(lax.axis_index(NEAR) * rows, rows), rows), :]
    spare = jnp.zeros((sequences - 1 - len(parts), head), F32)
    for s in range(sequences):
        total = jnp.zeros((rows, head), F32)
        for b in range(blocks):
            column = mine[:, b * sequences + s : b * sequences + s + 1]
            total = total + in_ref[order.index(b), s * rows : (s + 1) * rows, :] * column
        out_ref[far_ranks.index(s), :rows, :] = total
        out_ref[far_ranks.index(s), rows:, :] = jnp.concatenate(
            [later[s : s + 1], *(part[s : s + 1] for part in parts), spare], axis=0
        )


def far_kernel(order, in_ref, gap_ref, gain_ref, state_ref, part_ref, turned):
    blocks = in_ref.shape[0]
    rows, head = state_ref.shape
    later = jnp.zeros((1, head), F32)
    factors = [None] * blocks
    for b in reversed(range(blocks)):
        factors[b] = jnp.exp(later)
        later = later + in_ref[order.index(b), rows : rows + 1, :]
    tile = sum(in_ref[b, rows:, :] for b in range(blocks))
    query, forget, value, gate = (tile[k : k + 1] for k in range(1, 5))
    loss = gap_ref[...] * jax.nn.sigmoid(-forget)
    own = jnp.sum(query * loss, axis=1, keepdims=True) * value.astype(BF16).astype(F32)
    gate = gain_ref[...] * (gate * jax.nn.sigmoid(gate))
    weight = query * (1.0 - loss)
    rest = jnp.zeros((head - blocks - 1, head), F32)
    turned[...] = jnp.transpose(jnp.concatenate([*factors, weight, rest], axis=0))
    mine = turned[pl.ds(pl.multiple_of(lax.axis_index(NEAR) * rows, rows), rows), :]
    total = jnp.zeros((rows, head), F32)
    for b in range(blocks):
        total = total + in_ref[order.index(b), :rows, :] * mine[:, b : b + 1]
    state_ref[...] = total.astype(state_ref.dtype)
    part = jnp.sum(total * mine[:, blocks : blocks + 1], axis=0, keepdims=True)
    part = part + jnp.where(lax.axis_index(NEAR) == 0, own, 0.0)
    row = lax.broadcasted_iota(jnp.int32, part_ref.shape, 0)
    part_ref[...] = jnp.where(lax.rem(row, 2) == 0, part, gate)


def read_kernel(part_ref, state_ref, out_ref, cache_ref):
    cache_ref[...] = state_ref[...]
    sequences, head = out_ref.shape
    parts = part_ref[...].reshape(sequences, part_ref.shape[0] // sequences, head)
    row = lax.broadcasted_iota(jnp.int32, parts.shape, 1)
    mixed = jnp.sum(jnp.where(lax.rem(row, 2) == 0, parts, 0.0), axis=1)
    scale = lax.rsqrt(jnp.mean(mixed * mixed, axis=1, keepdims=True) + EPSILON)
    read = mixed * scale * parts[:, 1, :]
    places = [READ_ORDER.index(s) for s in range(sequences)]
    read = jnp.concatenate([read[a : a + 1] for a in places], axis=0)
    out_ref[...] = read.astype(out_ref.dtype)


def cost(flops, bytes_accessed):
    return pl.CostEstimate(flops=flops, bytes_accessed=bytes_accessed, transcendentals=0)


def exchanged(x, axes, ranks):
    return lax.all_to_all(x, axes, 0, 0, tiled=True, axis_index_groups=[ranks])


VMEM = pl.BlockSpec(memory_space=pltpu.VMEM)


def per_device(
    prompt, keep_scale, new_token, w_query, w_forget, w_value, w_outgate, floor_gap, norm_gain
):
    sequences, positions, width = prompt.shape
    head = norm_gain.shape[0]
    near = lax.axis_size(NEAR)
    far = lax.axis_size(HI)
    rows = head // near
    near_ranks = near_order(lax.axis_size(LO))
    far_ranks = list(FAR_ORDER)
    read_ranks = read_order(near_ranks)
    gap = floor_gap.reshape(1, head)
    gain = norm_gain.reshape(1, head)
    shaped = jax.ShapeDtypeStruct

    head_start = pl.pallas_call(
        opening_kernel,
        out_shape=shaped((8, head), F32),
        out_specs=VMEM,
        cost_estimate=cost(20_000_000_000, 40_000_000),
        name="opening",
        compiler_params=pltpu.CompilerParams(vmem_limit_bytes=1 << 20),
    )()
    token = lax.ppermute(new_token, (HI, TP), token_route(far, lax.axis_size(TP)))
    states = pl.pallas_call(
        functools.partial(state_kernel, near_ranks),
        out_shape=shaped((near, head + sequences, head), F32),
        in_specs=[VMEM] * 6,
        out_specs=VMEM,
        scratch_shapes=[pltpu.VMEM((sequences * positions, 2 * head), F32)],
        cost_estimate=cost(600_000_000, 4_000_000),
        name="block_states",
        compiler_params=pltpu.CompilerParams(vmem_limit_bytes=8 << 20),
    )(head_start, prompt, keep_scale, gap, w_forget, w_value)
    states = exchanged(states, NEAR, near_ranks)
    states = pl.pallas_call(
        functools.partial(near_kernel, near_ranks, far_ranks),
        out_shape=shaped((far, rows + sequences, head), F32),
        in_specs=[VMEM] * 6,
        out_specs=VMEM,
        scratch_shapes=[pltpu.VMEM((head, head), F32)],
        cost_estimate=cost(20_000_000, 2_600_000),
        name="near_states",
        compiler_params=pltpu.CompilerParams(vmem_limit_bytes=6 << 20),
    )(states, token, w_query, w_forget, w_value, w_outgate)
    states = exchanged(states, HI, far_ranks)
    final, part = pl.pallas_call(
        functools.partial(far_kernel, far_ranks),
        out_shape=(shaped((rows, head), BF16), shaped((2 * near * far, head), F32)),
        in_specs=[VMEM] * 3,
        out_specs=(VMEM,) * 2,
        scratch_shapes=[pltpu.VMEM((head, head), F32)],
        cost_estimate=cost(1_000_000, 200_000),
        name="far_states",
        compiler_params=pltpu.CompilerParams(vmem_limit_bytes=2 << 20),
    )(states, gap, gain)
    part = exchanged(part.reshape(near * far, 2, head), SP, read_ranks).reshape(part.shape)
    first_read, cache = pl.pallas_call(
        read_kernel,
        out_shape=(shaped((sequences, head), BF16), shaped((rows, head), BF16)),
        in_specs=[VMEM] * 2,
        out_specs=(VMEM,) * 2,
        cost_estimate=cost(100_000, 40_000),
        name="read",
        compiler_params=pltpu.CompilerParams(vmem_limit_bytes=1 << 20),
    )(part, final)
    return cache[None], first_read


def solution(mesh):
    finer = Mesh(mesh.devices.reshape(8, 2, 4, mesh.shape["tp"]), (HI, LO, Y, TP))
    placed = (
        P(None, SP, None),
        P(None, SP),
        P(None, TP),
        P(None, TP),
        P(None, TP),
        P(None, TP),
        P(None, TP),
        P(TP),
        P(),
    )
    return jax.shard_map(
        per_device,
        mesh=finer,
        in_specs=placed,
        out_specs=(P(TP, SP, None), P(None, TP)),
        check_vma=False,
    )
```

time: 64.6 us -> 63.1 us (0.977)
  the two profiles are of different devices: /device:TPU:8 before, /device:TPU:2 now
where the time goes in v5:
time: 63.1 us; the launch traced here: 62.9 us
  blocking collectives  41.3 us (65%)
  starting transfers between devices  7.88 us (12%)
  waiting for transfers between devices  7.09 us (11%)
  Pallas kernels  3.97 us (6%)
  local copies, waits for them, and re-layouts  1.92 us (3%)
  between operations  0.72 us (1%)
    all_to_all x2, blocking collectives, exchanged(): return lax.all_to_all(x, axes, 0, 0, tiled=True, axis_index_groups=[ranks])  41.3 us
    all_to_all x1, starting transfers between devices, exchanged(): return lax.all_to_all(x, axes, 0, 0, tiled=True, axis_index_groups=[ranks])  7.23 us
    all_to_all x1, waiting for transfers between devices, exchanged(): return lax.all_to_all(x, axes, 0, 0, tiled=True, axis_index_groups=[ranks])  7.09 us
    pallas_call x1, Pallas kernels, per_device(): pl.pallas_call(functools.partial(state_kernel, near_ranks), out_shape=sha...  2.63 us
    unnamed x18, local copies, waits for them, and re-layouts  1.92 us
  transfers between devices with their start and end apart: 2, of which 1 were waited for; matrix products, arithmetic and copies ran while one was open for 0% of the time, Pallas kernels for 0%

profile of v5, /device:TPU:2, one launch (start us, length us, event | category | flops | bytes accessed | tf_op | source)
XLA Modules:
  0.0 62.9 jit_solution(2834505162254893662)
XLA Ops:
  0.6 0.0 copy-start.6
  0.6 0.0 copy-start.5
  0.7 0.0 copy-start.1
  0.7 0.0 copy-start.2
  0.7 0.0 copy-start
  0.7 0.6 copy-done.6
  1.3 0.0 copy-done.5
  1.3 0.4 copy-done.1
  1.7 0.2 copy-done.2
  1.9 0.7 %copy-done = bf16[8,64,2048]{2,1,0:T(8,128)(2,1)S(1)} copy-done((bf16[8,64,2048]{2,1,0:T(8,128)(2,1)S(1)}, bf16[8,64,2048]{2,1,0:T(8,128)(2,1)}, u32[]{:S(2)}) %copy-start) | copy-done | bytes 2097176
  2.6 0.0 copy-start.8
  2.6 0.0 copy-start.3
  2.6 0.0 copy-start.4
  2.6 2.6 %block_states.1 = f32[8,136,128]{2,1,0:T(8,128)} custom-call(f32[8,128]{1,0:T(8,128)S(1)} %opening.1.opening_ref, bf16[8,64,2048]{2,1,0:T(8,128)(2,1)S(1)} %copy-done, f32[8,64]{1,0:T(8,128)S(1)} %copy-done.5, f32[1,128]{1,0:T(1,128)S(1)} %bitcast.7, bf16[2048,128]{1,0:T(8,128)(2,1)S(1)} %copy-done.1, bf16[2048,128]{1,0:T(8,128)(2,1)S(1)} %copy-done.2), custom_call_target="tpu_custom_call" | custom-call | flops 600000000 | bytes 4000000 | tf_op jit(solution)/shard_map/block_states/pallas_call | solution.py:210
  5.2 0.0 copy-start.7
  5.2 7.2 %all-to-all-start = ((f32[8,136,128]{2,1,0:T(8,128)}), f32[8,136,128]{2,1,0:T(8,128)S(1)}, u32[]{:S(2)}, u32[]{:S(2)}) async-start(f32[8,136,128]{2,1,0:T(8,128)} %block_states.1), calls=%async_computation | async-start | bytes 1114112 | tf_op jit(solution)/shard_map/all_to_all | solution.py:180
  12.5 0.0 copy-done.8
  12.5 0.7 %collective-permute-start = (bf16[8,256]{1,0:T(8,128)(2,1)S(1)}, bf16[8,256]{1,0:T(8,128)(2,1)S(1)}, u32[]{:S(2)}, u32[]{:S(2)}) collective-permute-start(bf16[8,256]{1,0:T(8,128)(2,1)S(1)} %copy-done.8), channel_id=1, source_target_pairs={{0,0},{1,1},{2,2},{3,3},{4,4},{5,5},{6,6},{7,7},{65,64},{66,65},{6... | collective-permute-start | bytes 12296 | tf_op jit(solution)/shard_map/ppermute | solution.py:209
  13.1 0.0 collective-permute-done.token_ref
  13.1 7.1 %all-to-all-done.in_ref = f32[8,136,128]{2,1,0:T(8,128)S(1)} async-done(((f32[8,136,128]{2,1,0:T(8,128)}), f32[8,136,128]{2,1,0:T(8,128)S(1)}, u32[]{:S(2)}, u32[]{:S(2)}) %all-to-all-start) | async-done | bytes 557088 | tf_op jit(solution)/shard_map/all_to_all | solution.py:180
  20.2 0.0 copy-done.3
  20.2 0.0 copy-done.4
  20.2 0.4 near_states.1
  20.6 22.4 %all_to_all.15.in_ref = f32[8,24,128]{2,1,0:T(8,128)S(1)} all-to-all(f32[8,24,128]{2,1,0:T(8,128)S(1)} %near_states.1), channel_id=1, replica_groups={{256,0,448,64,384,128,320,192},{257,1,449,65,385,129,321,193},{258,2,45..., dimensions={0} | all-to-all | bytes 196608 | tf_op jit(solution)/shard_map/all_to_all | solution.py:180
  43.0 0.0 copy-done.7
  43.0 0.2 far_states.1
  43.3 18.9 %all_to_all.16 = f32[64,2,128]{2,1,0:T(2,128)S(1)} all-to-all(f32[64,2,128]{2,1,0:T(2,128)S(1)} %bitcast.6), channel_id=1, replica_groups={{272,280,256,264,304,312,288,296,16,24,0,8,48,56,32,40,464,472,448,456,..., dimensions={0} | all-to-all | bytes 131072 | tf_op jit(solution)/shard_map/all_to_all | solution.py:180
  62.2 0.7 %read.1 = (bf16[8,128]{1,0:T(8,128)(2,1)}, bf16[16,128]{1,0:T(8,128)(2,1)}) custom-call(f32[128,128]{1,0:T(8,128)S(1)} %bitcast.5, bf16[16,128]{1,0:T(8,128)(2,1)S(1)} %get-tuple-element.7.state_ref), custom_call_target="tpu_custom_call" | custom-call | flops 100000 | bytes 40000 | tf_op jit(solution)/shard_map/read/pallas_call | solution.py:243
  (1 shorter events, 0.0 us)
Async XLA Ops:
  0.6 0.7 %copy-start.6 = (f32[128]{0:T(128)S(1)}, f32[128]{0:T(128)}, u32[]{:S(2)}) copy-start(f32[128]{0:T(128)} %param.16) | copy-start | bytes 1540
  0.6 0.7 %copy-start.5 = (f32[8,64]{1,0:T(8,128)S(1)}, f32[8,64]{1,0:T(8,128)}, u32[]{:S(2)}) copy-start(f32[8,64]{1,0:T(8,128)} %keep_ref.1) | copy-start | bytes 6148
  0.7 1.1 %copy-start.1 = (bf16[2048,128]{1,0:T(8,128)(2,1)S(1)}, bf16[2048,128]{1,0:T(8,128)(2,1)}, u32[]{:S(2)}) copy-start(bf16[2048,128]{1,0:T(8,128)(2,1)} %wf_ref.3) | copy-start | bytes 1572868
  0.7 1.2 %copy-start.2 = (bf16[2048,128]{1,0:T(8,128)(2,1)S(1)}, bf16[2048,128]{1,0:T(8,128)(2,1)}, u32[]{:S(2)}) copy-start(bf16[2048,128]{1,0:T(8,128)(2,1)} %wv_ref.3) | copy-start | bytes 1572868
  0.7 1.9 %copy-start = (bf16[8,64,2048]{2,1,0:T(8,128)(2,1)S(1)}, bf16[8,64,2048]{2,1,0:T(8,128)(2,1)}, u32[]{:S(2)}) copy-start(bf16[8,64,2048]{2,1,0:T(8,128)(2,1)} %prompt_ref.1) | copy-start | bytes 6291460
  2.6 9.9 %copy-start.8 = (bf16[8,256]{1,0:T(8,128)(2,1)S(1)}, bf16[8,256]{1,0:T(8,128)(2,1)}, u32[]{:S(2)}) copy-start(bf16[8,256]{1,0:T(8,128)(2,1)} %param.11) | copy-start | bytes 12292
  2.6 17.6 %copy-start.3 = (bf16[2048,128]{1,0:T(8,128)(2,1)S(1)}, bf16[2048,128]{1,0:T(8,128)(2,1)}, u32[]{:S(2)}) copy-start(bf16[2048,128]{1,0:T(8,128)(2,1)} %wq_ref.1) | copy-start | bytes 1572868
  2.6 17.6 %copy-start.4 = (bf16[2048,128]{1,0:T(8,128)(2,1)S(1)}, bf16[2048,128]{1,0:T(8,128)(2,1)}, u32[]{:S(2)}) copy-start(bf16[2048,128]{1,0:T(8,128)(2,1)} %wg_ref.1) | copy-start | bytes 1572868
  5.2 37.8 %copy-start.7 = (f32[128]{0:T(128)S(1)}, f32[128]{0:T(128)}, u32[]{:S(2)}) copy-start(f32[128]{0:T(128)} %param.17) | copy-start | bytes 1540
  5.2 15.0 %all-to-all-start = ((f32[8,136,128]{2,1,0:T(8,128)}), f32[8,136,128]{2,1,0:T(8,128)S(1)}, u32[]{:S(2)}, u32[]{:S(2)}) async-start(f32[8,136,128]{2,1,0:T(8,128)} %block_states.1), calls=%async_computation | async-start | bytes 1114112 | tf_op jit(solution)/shard_map/all_to_all | solution.py:180
  12.5 0.7 %collective-permute-start = (bf16[8,256]{1,0:T(8,128)(2,1)S(1)}, bf16[8,256]{1,0:T(8,128)(2,1)S(1)}, u32[]{:S(2)}, u32[]{:S(2)}) collective-permute-start(bf16[8,256]{1,0:T(8,128)(2,1)S(1)} %copy-done.8), channel_id=1, source_target_pairs={{0,0},{1,1},{2,2},{3,3},{4,4},{5,5},{6,6},{7,7},{65,64},{66,65},{6... | collective-permute-start | bytes 12296 | tf_op jit(solution)/shard_map/ppermute | solution.py:209

commit v6 on v5

--- a/solution.py
+++ b/solution.py
@@ -12,16 +12,9 @@
 SP = (HI, LO, Y)
 NEAR = (LO, Y)
 EPSILON = 1e-06
-
-
-FAR_ORDER, READ_ORDER, Y_ORDER = (4, 0, 7, 1, 6, 2, 5, 3), (4, 0, 7, 1, 6, 2, 5, 3), (2, 3, 0, 1)
-
-
 F32, BF16 = jnp.float32, jnp.bfloat16
-
-
-def near_order(low):
-    return [l * len(Y_ORDER) + m for l in range(low) for m in Y_ORDER]
+FAR_ORDER = READ_ORDER = (4, 0, 7, 1, 6, 2, 5, 3)
+NEAR_ORDER = (2, 0, 3, 1, 6, 4, 7, 5)
 
 
 def read_order(near):
@@ -191,7 +184,7 @@
     near = lax.axis_size(NEAR)
     far = lax.axis_size(HI)
     rows = head // near
-    near_ranks = near_order(lax.axis_size(LO))
+    near_ranks = list(NEAR_ORDER)
     far_ranks = list(FAR_ORDER)
     read_ranks = read_order(near_ranks)
     gap = floor_gap.reshape(1, head)
@@ -239,7 +232,7 @@
         name="far_states",
         compiler_params=pltpu.CompilerParams(vmem_limit_bytes=2 << 20),
     )(states, gap, gain)
-    part = exchanged(part.reshape(near * far, 2, head), SP, read_ranks).reshape(part.shape)
+    part = exchanged(part.reshape(near * far, 1, 2 * head), SP, read_ranks).reshape(part.shape)
     first_read, cache = pl.pallas_call(
         read_kernel,
         out_shape=(shaped((sequences, head), BF16), shaped((rows, head), BF16)),

time: 63.1 us -> 62.6 us (level)
  no operation moved by 1% of the time
where the time goes in v6:
time: 62.6 us; the launch traced here: 62.3 us
  blocking collectives  40.7 us (65%)
  starting transfers between devices  7.88 us (13%)
  waiting for transfers between devices  7.14 us (11%)
  Pallas kernels  3.97 us (6%)
  local copies, waits for them, and re-layouts  1.92 us (3%)
  between operations  0.72 us (1%)
    all_to_all x2, blocking collectives, exchanged(): return lax.all_to_all(x, axes, 0, 0, tiled=True, axis_index_groups=[ranks])  40.7 us
    all_to_all x1, starting transfers between devices, exchanged(): return lax.all_to_all(x, axes, 0, 0, tiled=True, axis_index_groups=[ranks])  7.23 us
    all_to_all x1, waiting for transfers between devices, exchanged(): return lax.all_to_all(x, axes, 0, 0, tiled=True, axis_index_groups=[ranks])  7.14 us
    pallas_call x1, Pallas kernels, per_device(): pl.pallas_call(functools.partial(state_kernel, near_ranks), out_shape=sha...  2.63 us
    unnamed x18, local copies, waits for them, and re-layouts  1.92 us
  transfers between devices with their start and end apart: 2, of which 1 were waited for; matrix products, arithmetic and copies ran while one was open for 0% of the time, Pallas kernels for 0%

profile of v6, /device:TPU:2, one launch (start us, length us, event | category | flops | bytes accessed | tf_op | source)
XLA Modules:
  0.0 62.3 jit_solution(12255860755330747345)
XLA Ops:
  0.6 0.0 copy-start.6
  0.6 0.0 copy-start.5
  0.7 0.0 copy-start.1
  0.7 0.0 copy-start.2
  0.7 0.0 copy-start
  0.7 0.6 copy-done.6
  1.3 0.0 copy-done.5
  1.3 0.4 copy-done.1
  1.7 0.2 copy-done.2
  1.9 0.7 %copy-done = bf16[8,64,2048]{2,1,0:T(8,128)(2,1)S(1)} copy-done((bf16[8,64,2048]{2,1,0:T(8,128)(2,1)S(1)}, bf16[8,64,2048]{2,1,0:T(8,128)(2,1)}, u32[]{:S(2)}) %copy-start) | copy-done | bytes 2097176
  2.6 0.0 copy-start.8
  2.6 0.0 copy-start.3
  2.6 0.0 copy-start.4
  2.6 2.6 %block_states.1 = f32[8,136,128]{2,1,0:T(8,128)} custom-call(f32[8,128]{1,0:T(8,128)S(1)} %opening.1.opening_ref, bf16[8,64,2048]{2,1,0:T(8,128)(2,1)S(1)} %copy-done, f32[8,64]{1,0:T(8,128)S(1)} %copy-done.5, f32[1,128]{1,0:T(1,128)S(1)} %bitcast.7, bf16[2048,128]{1,0:T(8,128)(2,1)S(1)} %copy-done.1, bf16[2048,128]{1,0:T(8,128)(2,1)S(1)} %copy-done.2), custom_call_target="tpu_custom_call" | custom-call | flops 600000000 | bytes 4000000 | tf_op jit(solution)/shard_map/block_states/pallas_call | solution.py:203
  5.2 0.0 copy-start.7
  5.2 7.2 %all-to-all-start = ((f32[8,136,128]{2,1,0:T(8,128)}), f32[8,136,128]{2,1,0:T(8,128)S(1)}, u32[]{:S(2)}, u32[]{:S(2)}) async-start(f32[8,136,128]{2,1,0:T(8,128)} %block_states.1), calls=%async_computation | async-start | bytes 1114112 | tf_op jit(solution)/shard_map/all_to_all | solution.py:173
  12.5 0.0 copy-done.8
  12.5 0.7 %collective-permute-start = (bf16[8,256]{1,0:T(8,128)(2,1)S(1)}, bf16[8,256]{1,0:T(8,128)(2,1)S(1)}, u32[]{:S(2)}, u32[]{:S(2)}) collective-permute-start(bf16[8,256]{1,0:T(8,128)(2,1)S(1)} %copy-done.8), channel_id=1, source_target_pairs={{0,0},{1,1},{2,2},{3,3},{4,4},{5,5},{6,6},{7,7},{65,64},{66,65},{6... | collective-permute-start | bytes 12296 | tf_op jit(solution)/shard_map/ppermute | solution.py:202
  13.1 0.0 collective-permute-done.token_ref
  13.1 7.1 %all-to-all-done.in_ref = f32[8,136,128]{2,1,0:T(8,128)S(1)} async-done(((f32[8,136,128]{2,1,0:T(8,128)}), f32[8,136,128]{2,1,0:T(8,128)S(1)}, u32[]{:S(2)}, u32[]{:S(2)}) %all-to-all-start) | async-done | bytes 557088 | tf_op jit(solution)/shard_map/all_to_all | solution.py:173
  20.3 0.0 copy-done.3
  20.3 0.0 copy-done.4
  20.3 0.4 near_states.1
  20.7 22.3 %all_to_all.15.in_ref = f32[8,24,128]{2,1,0:T(8,128)S(1)} all-to-all(f32[8,24,128]{2,1,0:T(8,128)S(1)} %near_states.1), channel_id=1, replica_groups={{256,0,448,64,384,128,320,192},{257,1,449,65,385,129,321,193},{258,2,45..., dimensions={0} | all-to-all | bytes 196608 | tf_op jit(solution)/shard_map/all_to_all | solution.py:173
  43.0 0.0 copy-done.7
  43.0 0.2 far_states.1
  43.2 18.4 %all_to_all.16 = f32[64,1,256]{2,1,0:T(1,128)S(1)} all-to-all(f32[64,1,256]{2,1,0:T(1,128)S(1)} %bitcast.6), channel_id=1, replica_groups={{272,256,280,264,304,288,312,296,16,0,24,8,48,32,56,40,464,448,472,456,..., dimensions={0} | all-to-all | bytes 131072 | tf_op jit(solution)/shard_map/all_to_all | solution.py:173
  61.6 0.7 %read.1 = (bf16[8,128]{1,0:T(8,128)(2,1)}, bf16[16,128]{1,0:T(8,128)(2,1)}) custom-call(f32[128,128]{1,0:T(8,128)S(1)} %bitcast.5, bf16[16,128]{1,0:T(8,128)(2,1)S(1)} %get-tuple-element.7.state_ref), custom_call_target="tpu_custom_call" | custom-call | flops 100000 | bytes 40000 | tf_op jit(solution)/shard_map/read/pallas_call | solution.py:236
  (1 shorter events, 0.0 us)
Async XLA Ops:
  0.6 0.7 %copy-start.6 = (f32[128]{0:T(128)S(1)}, f32[128]{0:T(128)}, u32[]{:S(2)}) copy-start(f32[128]{0:T(128)} %param.16) | copy-start | bytes 1540
  0.6 0.7 %copy-start.5 = (f32[8,64]{1,0:T(8,128)S(1)}, f32[8,64]{1,0:T(8,128)}, u32[]{:S(2)}) copy-start(f32[8,64]{1,0:T(8,128)} %keep_ref.1) | copy-start | bytes 6148
  0.7 1.1 %copy-start.1 = (bf16[2048,128]{1,0:T(8,128)(2,1)S(1)}, bf16[2048,128]{1,0:T(8,128)(2,1)}, u32[]{:S(2)}) copy-start(bf16[2048,128]{1,0:T(8,128)(2,1)} %wf_ref.3) | copy-start | bytes 1572868
  0.7 1.2 %copy-start.2 = (bf16[2048,128]{1,0:T(8,128)(2,1)S(1)}, bf16[2048,128]{1,0:T(8,128)(2,1)}, u32[]{:S(2)}) copy-start(bf16[2048,128]{1,0:T(8,128)(2,1)} %wv_ref.3) | copy-start | bytes 1572868
  0.7 1.9 %copy-start = (bf16[8,64,2048]{2,1,0:T(8,128)(2,1)S(1)}, bf16[8,64,2048]{2,1,0:T(8,128)(2,1)}, u32[]{:S(2)}) copy-start(bf16[8,64,2048]{2,1,0:T(8,128)(2,1)} %prompt_ref.1) | copy-start | bytes 6291460
  2.6 9.9 %copy-start.8 = (bf16[8,256]{1,0:T(8,128)(2,1)S(1)}, bf16[8,256]{1,0:T(8,128)(2,1)}, u32[]{:S(2)}) copy-start(bf16[8,256]{1,0:T(8,128)(2,1)} %param.11) | copy-start | bytes 12292
  2.6 17.7 %copy-start.3 = (bf16[2048,128]{1,0:T(8,128)(2,1)S(1)}, bf16[2048,128]{1,0:T(8,128)(2,1)}, u32[]{:S(2)}) copy-start(bf16[2048,128]{1,0:T(8,128)(2,1)} %wq_ref.1) | copy-start | bytes 1572868
  2.6 17.7 %copy-start.4 = (bf16[2048,128]{1,0:T(8,128)(2,1)S(1)}, bf16[2048,128]{1,0:T(8,128)(2,1)}, u32[]{:S(2)}) copy-start(bf16[2048,128]{1,0:T(8,128)(2,1)} %wg_ref.1) | copy-start | bytes 1572868
  5.2 37.7 %copy-start.7 = (f32[128]{0:T(128)S(1)}, f32[128]{0:T(128)}, u32[]{:S(2)}) copy-start(f32[128]{0:T(128)} %param.17) | copy-start | bytes 1540
  5.2 15.0 %all-to-all-start = ((f32[8,136,128]{2,1,0:T(8,128)}), f32[8,136,128]{2,1,0:T(8,128)S(1)}, u32[]{:S(2)}, u32[]{:S(2)}) async-start(f32[8,136,128]{2,1,0:T(8,128)} %block_states.1), calls=%async_computation | async-start | bytes 1114112 | tf_op jit(solution)/shard_map/all_to_all | solution.py:173
  12.5 0.7 %collective-permute-start = (bf16[8,256]{1,0:T(8,128)(2,1)S(1)}, bf16[8,256]{1,0:T(8,128)(2,1)S(1)}, u32[]{:S(2)}, u32[]{:S(2)}) collective-permute-start(bf16[8,256]{1,0:T(8,128)(2,1)S(1)} %copy-done.8), channel_id=1, source_target_pairs={{0,0},{1,1},{2,2},{3,3},{4,4},{5,5},{6,6},{7,7},{65,64},{66,65},{6... | collective-permute-start | bytes 12296 | tf_op jit(solution)/shard_map/ppermute | solution.py:202

commit v7 on v6

--- a/solution.py
+++ b/solution.py
@@ -7,6 +7,7 @@
 from jax.experimental.pallas import tpu as pltpu
 from jax.sharding import Mesh
 from jax.sharding import PartitionSpec as P
+
 
 HI, LO, Y, TP = "sp_hi", "sp_lo", "sp_y", "tp"
 SP = (HI, LO, Y)
@@ -88,23 +89,13 @@
 
 
 def token_route(far, tp):
-    return [(h * tp + (i + h) % tp, h * tp + i) for h in range(far) for i in range(tp)]
-
-
-def near_kernel(
-    order, far_ranks, in_ref, token_ref, wq_ref, wf_ref, wv_ref, wg_ref, out_ref, turned
-):
+    return [(h * tp + (i ^ h ^ (tp - 1)), h * tp + i) for h in range(far) for i in range(tp)]
+
+
+def near_kernel(order, far_ranks, in_ref, out_ref, later_ref, turned):
     blocks = in_ref.shape[0]
     sequences, _, head = out_ref.shape
     rows = head // blocks
-    width = token_ref.shape[1]
-    block = lax.rem(lax.axis_index(TP) + lax.axis_index(HI), lax.axis_size(TP))
-    span = pl.ds(pl.multiple_of(block * width, width), width)
-    token = token_ref[...]
-    parts = [
-        jnp.dot(token, ref[span, :], preferred_element_type=F32)
-        for ref in (wq_ref, wf_ref, wv_ref, wg_ref)
-    ]
     later = jnp.zeros((sequences, head), F32)
     factors = [None] * blocks
     for b in reversed(range(blocks)):
@@ -113,16 +104,38 @@
     rest = jnp.zeros((head - blocks * sequences, head), F32)
     turned[...] = jnp.transpose(jnp.concatenate([*factors, rest], axis=0))
     mine = turned[pl.ds(pl.multiple_of(lax.axis_index(NEAR) * rows, rows), rows), :]
-    spare = jnp.zeros((sequences - 1 - len(parts), head), F32)
+    later_ref[...] = later
     for s in range(sequences):
         total = jnp.zeros((rows, head), F32)
         for b in range(blocks):
             column = mine[:, b * sequences + s : b * sequences + s + 1]
             total = total + in_ref[order.index(b), s * rows : (s + 1) * rows, :] * column
         out_ref[far_ranks.index(s), :rows, :] = total
-        out_ref[far_ranks.index(s), rows:, :] = jnp.concatenate(
-            [later[s : s + 1], *(part[s : s + 1] for part in parts), spare], axis=0
+
+
+def token_kernel(
+    far_ranks, token_ref, later_ref, wq_ref, wf_ref, wv_ref, wg_ref, states_ref, out_ref,
+    tile_buf, sem,
+):
+    del states_ref
+    width = token_ref.shape[1]
+    block = lax.axis_index(TP) ^ lax.axis_index(HI) ^ (lax.axis_size(TP) - 1)
+    span = pl.ds(pl.multiple_of(block * width, width), width)
+    token = token_ref[...]
+    parts = [later_ref[...]] + [
+        jnp.dot(token, ref[span, :], preferred_element_type=F32)
+        for ref in (wq_ref, wf_ref, wv_ref, wg_ref)
+    ]
+    targets, tile_rows, head = tile_buf.shape
+    spare = jnp.zeros((tile_rows - len(parts), head), F32)
+    for s in range(targets):
+        tile_buf[far_ranks.index(s)] = jnp.concatenate(
+            [*(part[s : s + 1] for part in parts), spare], axis=0
         )
+    last = pl.ds(out_ref.shape[1] - tile_rows, tile_rows)
+    copy = pltpu.make_async_copy(tile_buf, out_ref.at[:, last], sem)
+    copy.start()
+    copy.wait()
 
 
 def far_kernel(order, in_ref, gap_ref, gain_ref, state_ref, part_ref, turned):
@@ -173,13 +186,14 @@
     return lax.all_to_all(x, axes, 0, 0, tiled=True, axis_index_groups=[ranks])
 
 
+ANY = pl.BlockSpec(memory_space=pl.ANY)
 VMEM = pl.BlockSpec(memory_space=pltpu.VMEM)
 
 
-def per_device(
+def device_step(
     prompt, keep_scale, new_token, w_query, w_forget, w_value, w_outgate, floor_gap, norm_gain
 ):
-    sequences, positions, width = prompt.shape
+    sequences, positions, _ = prompt.shape
     head = norm_gain.shape[0]
     near = lax.axis_size(NEAR)
     far = lax.axis_size(HI)
@@ -211,16 +225,30 @@
         compiler_params=pltpu.CompilerParams(vmem_limit_bytes=8 << 20),
     )(head_start, prompt, keep_scale, gap, w_forget, w_value)
     states = exchanged(states, NEAR, near_ranks)
+    states, later = pl.pallas_call(
+        functools.partial(near_kernel, near_ranks, far_ranks),
+        out_shape=(
+            shaped((far, rows + sequences, head), F32),
+            shaped((sequences, head), F32),
+        ),
+        in_specs=[VMEM],
+        out_specs=(VMEM,) * 2,
+        scratch_shapes=[pltpu.VMEM((head, head), F32)],
+        cost_estimate=cost(1_000_000, 600_000),
+        name="near_states",
+        compiler_params=pltpu.CompilerParams(vmem_limit_bytes=2 << 20),
+    )(states)
     states = pl.pallas_call(
-        functools.partial(near_kernel, near_ranks, far_ranks),
-        out_shape=shaped((far, rows + sequences, head), F32),
-        in_specs=[VMEM] * 6,
-        out_specs=VMEM,
-        scratch_shapes=[pltpu.VMEM((head, head), F32)],
-        cost_estimate=cost(20_000_000, 2_600_000),
-        name="near_states",
+        functools.partial(token_kernel, far_ranks),
+        out_shape=shaped(states.shape, F32),
+        in_specs=[VMEM] * 6 + [ANY],
+        out_specs=ANY,
+        scratch_shapes=[pltpu.VMEM((far, sequences, head), F32), pltpu.SemaphoreType.DMA],
+        input_output_aliases={6: 0},
+        cost_estimate=cost(20_000_000, 2_200_000),
+        name="token",
         compiler_params=pltpu.CompilerParams(vmem_limit_bytes=6 << 20),
-    )(states, token, w_query, w_forget, w_value, w_outgate)
+    )(token, later, w_query, w_forget, w_value, w_outgate, states)
     states = exchanged(states, HI, far_ranks)
     final, part = pl.pallas_call(
         functools.partial(far_kernel, far_ranks),
@@ -259,7 +287,7 @@
         P(),
     )
     return jax.shard_map(
-        per_device,
+        device_step,
         mesh=finer,
         in_specs=placed,
         out_specs=(P(TP, SP, None), P(None, TP)),

time: 62.6 us -> 62.8 us (level)
  starting transfers between devices: 7.88 us -> 9.5 us
  waiting for transfers between devices: 7.14 us -> 5.53 us
    ppermute x1, starting transfers between devices: 0.65 us -> 2.27 us  [device_step(): lax.ppermute(new_token, (HI, TP), token_route(far, lax.axis_size(TP)))]
    all_to_all x1, waiting for transfers between devices: 7.14 us -> 5.53 us  [exchanged(): return lax.all_to_all(x, axes, 0, 0, tiled=True, axis_index_groups=[ranks])]
    pallas_call x5 -> x6, Pallas kernels: 3.97 us -> 4.16 us  [the longest x1 2.64 us: device_step(): pl.pallas_call(functools.partial(state_kernel, near_ranks), out_shape=sha...]
  transfers between devices with their start and end apart: 2 -> 2, of which waited for: 1 -> 1; matrix products, arithmetic and copies ran while one was open for 0% -> 0% of each run, Pallas kernels for 0% -> 1%
where the time goes in v7:
time: 62.8 us; the launch traced here: 62.5 us
  blocking collectives  40.7 us (65%)
  starting transfers between devices  9.5 us (15%)
  waiting for transfers between devices  5.53 us (9%)
  Pallas kernels  4.16 us (7%)
  local copies, waits for them, and re-layouts  1.92 us (3%)
  between operations  0.74 us (1%)
    all_to_all x2, blocking collectives, exchanged(): return lax.all_to_all(x, axes, 0, 0, tiled=True, axis_index_groups=[ranks])  40.7 us
    all_to_all x1, starting transfers between devices, exchanged(): return lax.all_to_all(x, axes, 0, 0, tiled=True, axis_index_groups=[ranks])  7.23 us
    all_to_all x1, waiting for transfers between devices, exchanged(): return lax.all_to_all(x, axes, 0, 0, tiled=True, axis_index_groups=[ranks])  5.53 us
    pallas_call x1, Pallas kernels, device_step(): pl.pallas_call(functools.partial(state_kernel, near_ranks), out_shape=sha...  2.64 us
    ppermute x1, starting transfers between devices, device_step(): lax.ppermute(new_token, (HI, TP), token_route(far, lax.axis_size(TP)))  2.27 us
    unnamed x18, local copies, waits for them, and re-layouts  1.92 us
  transfers between devices with their start and end apart: 2, of which 1 were waited for; matrix products, arithmetic and copies ran while one was open for 0% of the time, Pallas kernels for 1%

profile of v7, /device:TPU:2, one launch (start us, length us, event | category | flops | bytes accessed | tf_op | source)
XLA Modules:
  0.0 62.5 jit_solution(16275870974098559407)
XLA Ops:
  0.6 0.0 copy-start.6
  0.6 0.0 copy-start.5
  0.7 0.0 copy-start.1
  0.7 0.0 copy-start.2
  0.7 0.0 copy-start
  0.7 0.6 copy-done.6
  1.3 0.0 copy-done.5
  1.3 0.4 copy-done.1
  1.7 0.2 copy-done.2
  1.9 0.7 %copy-done = bf16[8,64,2048]{2,1,0:T(8,128)(2,1)S(1)} copy-done((bf16[8,64,2048]{2,1,0:T(8,128)(2,1)S(1)}, bf16[8,64,2048]{2,1,0:T(8,128)(2,1)}, u32[]{:S(2)}) %copy-start) | copy-done | bytes 2097176
  2.6 0.0 copy-start.8
  2.6 0.0 copy-start.3
  2.6 0.0 copy-start.4
  2.6 2.6 %block_states.1 = f32[8,136,128]{2,1,0:T(8,128)} custom-call(f32[8,128]{1,0:T(8,128)S(1)} %opening.1.opening_ref, bf16[8,64,2048]{2,1,0:T(8,128)(2,1)S(1)} %copy-done, f32[8,64]{1,0:T(8,128)S(1)} %copy-done.5, f32[1,128]{1,0:T(1,128)S(1)} %bitcast.7, bf16[2048,128]{1,0:T(8,128)(2,1)S(1)} %copy-done.1, bf16[2048,128]{1,0:T(8,128)(2,1)S(1)} %copy-done.2), custom_call_target="tpu_custom_call" | custom-call | flops 600000000 | bytes 4000000 | tf_op jit(solution)/shard_map/block_states/pallas_call | solution.py:217
  5.2 0.0 copy-start.7
  5.2 7.2 %all-to-all-start = ((f32[8,136,128]{2,1,0:T(8,128)}), f32[8,136,128]{2,1,0:T(8,128)S(1)}, u32[]{:S(2)}, u32[]{:S(2)}) async-start(f32[8,136,128]{2,1,0:T(8,128)} %block_states.1), calls=%async_computation | async-start | bytes 1114112 | tf_op jit(solution)/shard_map/all_to_all | solution.py:186
  12.5 0.0 copy-done.8
  12.5 2.3 %collective-permute-start = (bf16[8,256]{1,0:T(8,128)(2,1)S(1)}, bf16[8,256]{1,0:T(8,128)(2,1)S(1)}, u32[]{:S(2)}, u32[]{:S(2)}) collective-permute-start(bf16[8,256]{1,0:T(8,128)(2,1)S(1)} %copy-done.8), channel_id=1, source_target_pairs={{7,0},{6,1},{5,2},{4,3},{3,4},{2,5},{1,6},{0,7},{70,64},{71,65},{6... | collective-permute-start | bytes 12296 | tf_op jit(solution)/shard_map/ppermute | solution.py:216
  14.8 5.5 %all-to-all-done.in_ref = f32[8,136,128]{2,1,0:T(8,128)S(1)} async-done(((f32[8,136,128]{2,1,0:T(8,128)}), f32[8,136,128]{2,1,0:T(8,128)S(1)}, u32[]{:S(2)}, u32[]{:S(2)}) %all-to-all-start) | async-done | bytes 557088 | tf_op jit(solution)/shard_map/all_to_all | solution.py:186
  20.3 0.4 near_states.1
  20.7 0.0 collective-permute-done.token_ref
  20.7 0.0 copy-done.3
  20.7 0.0 copy-done.4
  20.7 0.2 token_.1
  20.9 22.3 %all_to_all.15.in_ref = f32[8,24,128]{2,1,0:T(8,128)S(1)} all-to-all(f32[8,24,128]{2,1,0:T(8,128)S(1)} %token_.1), channel_id=1, replica_groups={{256,0,448,64,384,128,320,192},{257,1,449,65,385,129,321,193},{258,2,45..., dimensions={0} | all-to-all | bytes 196608 | tf_op jit(solution)/shard_map/all_to_all | solution.py:186
  43.2 0.0 copy-done.7
  43.2 0.2 far_states.1
  43.4 18.4 %all_to_all.16 = f32[64,1,256]{2,1,0:T(1,128)S(1)} all-to-all(f32[64,1,256]{2,1,0:T(1,128)S(1)} %bitcast.6), channel_id=1, replica_groups={{272,256,280,264,304,288,312,296,16,0,24,8,48,32,56,40,464,448,472,456,..., dimensions={0} | all-to-all | bytes 131072 | tf_op jit(solution)/shard_map/all_to_all | solution.py:186
  61.8 0.7 %read.1 = (bf16[8,128]{1,0:T(8,128)(2,1)}, bf16[16,128]{1,0:T(8,128)(2,1)}) custom-call(f32[128,128]{1,0:T(8,128)S(1)} %bitcast.5, bf16[16,128]{1,0:T(8,128)(2,1)S(1)} %get-tuple-element.11.state_ref), custom_call_target="tpu_custom_call" | custom-call | flops 100000 | bytes 40000 | tf_op jit(solution)/shard_map/read/pallas_call | solution.py:264
  (1 shorter events, 0.0 us)
Async XLA Ops:
  0.6 0.7 %copy-start.6 = (f32[128]{0:T(128)S(1)}, f32[128]{0:T(128)}, u32[]{:S(2)}) copy-start(f32[128]{0:T(128)} %param.16) | copy-start | bytes 1540
  0.6 0.7 %copy-start.5 = (f32[8,64]{1,0:T(8,128)S(1)}, f32[8,64]{1,0:T(8,128)}, u32[]{:S(2)}) copy-start(f32[8,64]{1,0:T(8,128)} %keep_ref.1) | copy-start | bytes 6148
  0.7 1.1 %copy-start.1 = (bf16[2048,128]{1,0:T(8,128)(2,1)S(1)}, bf16[2048,128]{1,0:T(8,128)(2,1)}, u32[]{:S(2)}) copy-start(bf16[2048,128]{1,0:T(8,128)(2,1)} %wf_ref.3) | copy-start | bytes 1572868
  0.7 1.2 %copy-start.2 = (bf16[2048,128]{1,0:T(8,128)(2,1)S(1)}, bf16[2048,128]{1,0:T(8,128)(2,1)}, u32[]{:S(2)}) copy-start(bf16[2048,128]{1,0:T(8,128)(2,1)} %wv_ref.3) | copy-start | bytes 1572868
  0.7 1.9 %copy-start = (bf16[8,64,2048]{2,1,0:T(8,128)(2,1)S(1)}, bf16[8,64,2048]{2,1,0:T(8,128)(2,1)}, u32[]{:S(2)}) copy-start(bf16[8,64,2048]{2,1,0:T(8,128)(2,1)} %prompt_ref.1) | copy-start | bytes 6291460
  2.6 9.9 %copy-start.8 = (bf16[8,256]{1,0:T(8,128)(2,1)S(1)}, bf16[8,256]{1,0:T(8,128)(2,1)}, u32[]{:S(2)}) copy-start(bf16[8,256]{1,0:T(8,128)(2,1)} %param.11) | copy-start | bytes 12292
  2.6 18.1 %copy-start.3 = (bf16[2048,128]{1,0:T(8,128)(2,1)S(1)}, bf16[2048,128]{1,0:T(8,128)(2,1)}, u32[]{:S(2)}) copy-start(bf16[2048,128]{1,0:T(8,128)(2,1)} %wq_ref.1) | copy-start | bytes 1572868
  2.6 18.1 %copy-start.4 = (bf16[2048,128]{1,0:T(8,128)(2,1)S(1)}, bf16[2048,128]{1,0:T(8,128)(2,1)}, u32[]{:S(2)}) copy-start(bf16[2048,128]{1,0:T(8,128)(2,1)} %wg_ref.1) | copy-start | bytes 1572868
  5.2 38.0 %copy-start.7 = (f32[128]{0:T(128)S(1)}, f32[128]{0:T(128)}, u32[]{:S(2)}) copy-start(f32[128]{0:T(128)} %param.17) | copy-start | bytes 1540
  5.2 15.0 %all-to-all-start = ((f32[8,136,128]{2,1,0:T(8,128)}), f32[8,136,128]{2,1,0:T(8,128)S(1)}, u32[]{:S(2)}, u32[]{:S(2)}) async-start(f32[8,136,128]{2,1,0:T(8,128)} %block_states.1), calls=%async_computation | async-start | bytes 1114112 | tf_op jit(solution)/shard_map/all_to_all | solution.py:186
  12.5 8.2 %collective-permute-start = (bf16[8,256]{1,0:T(8,128)(2,1)S(1)}, bf16[8,256]{1,0:T(8,128)(2,1)S(1)}, u32[]{:S(2)}, u32[]{:S(2)}) collective-permute-start(bf16[8,256]{1,0:T(8,128)(2,1)S(1)} %copy-done.8), channel_id=1, source_target_pairs={{7,0},{6,1},{5,2},{4,3},{3,4},{2,5},{1,6},{0,7},{70,64},{71,65},{6... | collective-permute-start | bytes 12296 | tf_op jit(solution)/shard_map/ppermute | solution.py:216

commit v8 on v7

--- a/solution.py
+++ b/solution.py
@@ -88,8 +88,12 @@
                 out_ref[r, head + s : head + s + 1, :] = total
 
 
+def route_mask(h, far):
+    return h ^ (far - 1) ^ (2 * (h < far // 2))
+
+
 def token_route(far, tp):
-    return [(h * tp + (i ^ h ^ (tp - 1)), h * tp + i) for h in range(far) for i in range(tp)]
+    return [(h * tp + (i ^ route_mask(h, far)), h * tp + i) for h in range(far) for i in range(tp)]
 
 
 def near_kernel(order, far_ranks, in_ref, out_ref, later_ref, turned):
@@ -119,7 +123,7 @@
 ):
     del states_ref
     width = token_ref.shape[1]
-    block = lax.axis_index(TP) ^ lax.axis_index(HI) ^ (lax.axis_size(TP) - 1)
+    block = lax.axis_index(TP) ^ route_mask(lax.axis_index(HI), lax.axis_size(HI))
     span = pl.ds(pl.multiple_of(block * width, width), width)
     token = token_ref[...]
     parts = [later_ref[...]] + [

time: 62.8 us -> 62.8 us (level)
  waiting for transfers between devices: 5.53 us -> 4.9 us
    ppermute x1, starting transfers between devices: 2.27 us -> 2.9 us  [device_step(): lax.ppermute(new_token, (HI, TP), token_route(far, lax.axis_size(TP)))]
    all_to_all x1, waiting for transfers between devices: 5.53 us -> 4.9 us  [exchanged(): return lax.all_to_all(x, axes, 0, 0, tiled=True, axis_index_groups=[ranks])]
where the time goes in v8:
time: 62.8 us; the launch traced here: 62.5 us
  blocking collectives  40.7 us (65%)
  starting transfers between devices  10.1 us (16%)
  waiting for transfers between devices  4.9 us (8%)
  Pallas kernels  4.17 us (7%)
  local copies, waits for them, and re-layouts  1.92 us (3%)
  between operations  0.74 us (1%)
    all_to_all x2, blocking collectives, exchanged(): return lax.all_to_all(x, axes, 0, 0, tiled=True, axis_index_groups=[ranks])  40.7 us
    all_to_all x1, starting transfers between devices, exchanged(): return lax.all_to_all(x, axes, 0, 0, tiled=True, axis_index_groups=[ranks])  7.23 us
    all_to_all x1, waiting for transfers between devices, exchanged(): return lax.all_to_all(x, axes, 0, 0, tiled=True, axis_index_groups=[ranks])  4.9 us
    ppermute x1, starting transfers between devices, device_step(): lax.ppermute(new_token, (HI, TP), token_route(far, lax.axis_size(TP)))  2.9 us
    pallas_call x1, Pallas kernels, device_step(): pl.pallas_call(functools.partial(state_kernel, near_ranks), out_shape=sha...  2.64 us
    unnamed x18, local copies, waits for them, and re-layouts  1.92 us
  transfers between devices with their start and end apart: 2, of which 1 were waited for; matrix products, arithmetic and copies ran while one was open for 0% of the time, Pallas kernels for 1%

profile of v8, /device:TPU:2, one launch (start us, length us, event | category | flops | bytes accessed | tf_op | source)
XLA Modules:
  0.0 62.5 jit_solution(2065623360371346356)
XLA Ops:
  0.6 0.0 copy-start.6
  0.6 0.0 copy-start.5
  0.7 0.0 copy-start.1
  0.7 0.0 copy-start.2
  0.7 0.0 copy-start
  0.7 0.6 copy-done.6
  1.3 0.0 copy-done.5
  1.3 0.4 copy-done.1
  1.7 0.2 copy-done.2
  1.9 0.7 %copy-done = bf16[8,64,2048]{2,1,0:T(8,128)(2,1)S(1)} copy-done((bf16[8,64,2048]{2,1,0:T(8,128)(2,1)S(1)}, bf16[8,64,2048]{2,1,0:T(8,128)(2,1)}, u32[]{:S(2)}) %copy-start) | copy-done | bytes 2097176
  2.6 0.0 copy-start.8
  2.6 0.0 copy-start.3
  2.6 0.0 copy-start.4
  2.6 2.6 %block_states.1 = f32[8,136,128]{2,1,0:T(8,128)} custom-call(f32[8,128]{1,0:T(8,128)S(1)} %opening.1.opening_ref, bf16[8,64,2048]{2,1,0:T(8,128)(2,1)S(1)} %copy-done, f32[8,64]{1,0:T(8,128)S(1)} %copy-done.5, f32[1,128]{1,0:T(1,128)S(1)} %bitcast.7, bf16[2048,128]{1,0:T(8,128)(2,1)S(1)} %copy-done.1, bf16[2048,128]{1,0:T(8,128)(2,1)S(1)} %copy-done.2), custom_call_target="tpu_custom_call" | custom-call | flops 600000000 | bytes 4000000 | tf_op jit(solution)/shard_map/block_states/pallas_call | solution.py:221
  5.2 0.0 copy-start.7
  5.2 7.2 %all-to-all-start = ((f32[8,136,128]{2,1,0:T(8,128)}), f32[8,136,128]{2,1,0:T(8,128)S(1)}, u32[]{:S(2)}, u32[]{:S(2)}) async-start(f32[8,136,128]{2,1,0:T(8,128)} %block_states.1), calls=%async_computation | async-start | bytes 1114112 | tf_op jit(solution)/shard_map/all_to_all | solution.py:190
  12.5 0.0 copy-done.8
  12.5 2.9 %collective-permute-start = (bf16[8,256]{1,0:T(8,128)(2,1)S(1)}, bf16[8,256]{1,0:T(8,128)(2,1)S(1)}, u32[]{:S(2)}, u32[]{:S(2)}) collective-permute-start(bf16[8,256]{1,0:T(8,128)(2,1)S(1)} %copy-done.8), channel_id=1, source_target_pairs={{5,0},{4,1},{7,2},{6,3},{1,4},{0,5},{3,6},{2,7},{68,64},{69,65},{7... | collective-permute-start | bytes 12296 | tf_op jit(solution)/shard_map/ppermute | solution.py:220
  15.4 4.9 %all-to-all-done.in_ref = f32[8,136,128]{2,1,0:T(8,128)S(1)} async-done(((f32[8,136,128]{2,1,0:T(8,128)}), f32[8,136,128]{2,1,0:T(8,128)S(1)}, u32[]{:S(2)}, u32[]{:S(2)}) %all-to-all-start) | async-done | bytes 557088 | tf_op jit(solution)/shard_map/all_to_all | solution.py:190
  20.3 0.4 near_states.1
  20.7 0.0 collective-permute-done.token_ref
  20.7 0.0 copy-done.3
  20.7 0.0 copy-done.4
  20.7 0.2 token_.1
  20.9 22.3 %all_to_all.15.in_ref = f32[8,24,128]{2,1,0:T(8,128)S(1)} all-to-all(f32[8,24,128]{2,1,0:T(8,128)S(1)} %token_.1), channel_id=1, replica_groups={{256,0,448,64,384,128,320,192},{257,1,449,65,385,129,321,193},{258,2,45..., dimensions={0} | all-to-all | bytes 196608 | tf_op jit(solution)/shard_map/all_to_all | solution.py:190
  43.2 0.0 copy-done.7
  43.2 0.2 far_states.1
  43.4 18.4 %all_to_all.16 = f32[64,1,256]{2,1,0:T(1,128)S(1)} all-to-all(f32[64,1,256]{2,1,0:T(1,128)S(1)} %bitcast.6), channel_id=1, replica_groups={{272,256,280,264,304,288,312,296,16,0,24,8,48,32,56,40,464,448,472,456,..., dimensions={0} | all-to-all | bytes 131072 | tf_op jit(solution)/shard_map/all_to_all | solution.py:190
  61.8 0.7 %read.1 = (bf16[8,128]{1,0:T(8,128)(2,1)}, bf16[16,128]{1,0:T(8,128)(2,1)}) custom-call(f32[128,128]{1,0:T(8,128)S(1)} %bitcast.5, bf16[16,128]{1,0:T(8,128)(2,1)S(1)} %get-tuple-element.11.state_ref), custom_call_target="tpu_custom_call" | custom-call | flops 100000 | bytes 40000 | tf_op jit(solution)/shard_map/read/pallas_call | solution.py:268
  (1 shorter events, 0.0 us)
Async XLA Ops:
  0.6 0.7 %copy-start.6 = (f32[128]{0:T(128)S(1)}, f32[128]{0:T(128)}, u32[]{:S(2)}) copy-start(f32[128]{0:T(128)} %param.16) | copy-start | bytes 1540
  0.6 0.7 %copy-start.5 = (f32[8,64]{1,0:T(8,128)S(1)}, f32[8,64]{1,0:T(8,128)}, u32[]{:S(2)}) copy-start(f32[8,64]{1,0:T(8,128)} %keep_ref.1) | copy-start | bytes 6148
  0.7 1.1 %copy-start.1 = (bf16[2048,128]{1,0:T(8,128)(2,1)S(1)}, bf16[2048,128]{1,0:T(8,128)(2,1)}, u32[]{:S(2)}) copy-start(bf16[2048,128]{1,0:T(8,128)(2,1)} %wf_ref.3) | copy-start | bytes 1572868
  0.7 1.2 %copy-start.2 = (bf16[2048,128]{1,0:T(8,128)(2,1)S(1)}, bf16[2048,128]{1,0:T(8,128)(2,1)}, u32[]{:S(2)}) copy-start(bf16[2048,128]{1,0:T(8,128)(2,1)} %wv_ref.3) | copy-start | bytes 1572868
  0.7 1.9 %copy-start = (bf16[8,64,2048]{2,1,0:T(8,128)(2,1)S(1)}, bf16[8,64,2048]{2,1,0:T(8,128)(2,1)}, u32[]{:S(2)}) copy-start(bf16[8,64,2048]{2,1,0:T(8,128)(2,1)} %prompt_ref.1) | copy-start | bytes 6291460
  2.6 9.9 %copy-start.8 = (bf16[8,256]{1,0:T(8,128)(2,1)S(1)}, bf16[8,256]{1,0:T(8,128)(2,1)}, u32[]{:S(2)}) copy-start(bf16[8,256]{1,0:T(8,128)(2,1)} %param.11) | copy-start | bytes 12292
  2.6 18.1 %copy-start.3 = (bf16[2048,128]{1,0:T(8,128)(2,1)S(1)}, bf16[2048,128]{1,0:T(8,128)(2,1)}, u32[]{:S(2)}) copy-start(bf16[2048,128]{1,0:T(8,128)(2,1)} %wq_ref.1) | copy-start | bytes 1572868
  2.6 18.1 %copy-start.4 = (bf16[2048,128]{1,0:T(8,128)(2,1)S(1)}, bf16[2048,128]{1,0:T(8,128)(2,1)}, u32[]{:S(2)}) copy-start(bf16[2048,128]{1,0:T(8,128)(2,1)} %wg_ref.1) | copy-start | bytes 1572868
  5.2 38.0 %copy-start.7 = (f32[128]{0:T(128)S(1)}, f32[128]{0:T(128)}, u32[]{:S(2)}) copy-start(f32[128]{0:T(128)} %param.17) | copy-start | bytes 1540
  5.2 15.0 %all-to-all-start = ((f32[8,136,128]{2,1,0:T(8,128)}), f32[8,136,128]{2,1,0:T(8,128)S(1)}, u32[]{:S(2)}, u32[]{:S(2)}) async-start(f32[8,136,128]{2,1,0:T(8,128)} %block_states.1), calls=%async_computation | async-start | bytes 1114112 | tf_op jit(solution)/shard_map/all_to_all | solution.py:190
  12.5 8.2 %collective-permute-start = (bf16[8,256]{1,0:T(8,128)(2,1)S(1)}, bf16[8,256]{1,0:T(8,128)(2,1)S(1)}, u32[]{:S(2)}, u32[]{:S(2)}) collective-permute-start(bf16[8,256]{1,0:T(8,128)(2,1)S(1)} %copy-done.8), channel_id=1, source_target_pairs={{5,0},{4,1},{7,2},{6,3},{1,4},{0,5},{3,6},{2,7},{68,64},{69,65},{7... | collective-permute-start | bytes 12296 | tf_op jit(solution)/shard_map/ppermute | solution.py:220

commit v9 on v6

--- a/solution.py
+++ b/solution.py
@@ -7,6 +7,7 @@
 from jax.experimental.pallas import tpu as pltpu
 from jax.sharding import Mesh
 from jax.sharding import PartitionSpec as P
+
 
 HI, LO, Y, TP = "sp_hi", "sp_lo", "sp_y", "tp"
 SP = (HI, LO, Y)
@@ -88,7 +89,7 @@
 
 
 def token_route(far, tp):
-    return [(h * tp + (i + h) % tp, h * tp + i) for h in range(far) for i in range(tp)]
+    return [(h * tp + (i ^ h ^ (tp - 1)), h * tp + i) for h in range(far) for i in range(tp)]
 
 
 def near_kernel(
@@ -98,7 +99,7 @@
     sequences, _, head = out_ref.shape
     rows = head // blocks
     width = token_ref.shape[1]
-    block = lax.rem(lax.axis_index(TP) + lax.axis_index(HI), lax.axis_size(TP))
+    block = lax.axis_index(TP) ^ lax.axis_index(HI) ^ (lax.axis_size(TP) - 1)
     span = pl.ds(pl.multiple_of(block * width, width), width)
     token = token_ref[...]
     parts = [
@@ -176,10 +177,10 @@
 VMEM = pl.BlockSpec(memory_space=pltpu.VMEM)
 
 
-def per_device(
+def device_step(
     prompt, keep_scale, new_token, w_query, w_forget, w_value, w_outgate, floor_gap, norm_gain
 ):
-    sequences, positions, width = prompt.shape
+    sequences, positions, _ = prompt.shape
     head = norm_gain.shape[0]
     near = lax.axis_size(NEAR)
     far = lax.axis_size(HI)
@@ -210,6 +211,7 @@
         name="block_states",
         compiler_params=pltpu.CompilerParams(vmem_limit_bytes=8 << 20),
     )(head_start, prompt, keep_scale, gap, w_forget, w_value)
+    states, token = lax.optimization_barrier((states, token))
     states = exchanged(states, NEAR, near_ranks)
     states = pl.pallas_call(
         functools.partial(near_kernel, near_ranks, far_ranks),
@@ -259,7 +261,7 @@
         P(),
     )
     return jax.shard_map(
-        per_device,
+        device_step,
         mesh=finer,
         in_specs=placed,
         out_specs=(P(TP, SP, None), P(None, TP)),

time: 62.6 us -> 61.4 us (0.981)
  blocking collectives: 40.7 us -> 53.8 us
  waiting for transfers between devices: 7.14 us -> 0.36 us
  starting transfers between devices: 7.88 us -> 3.1 us
  local copies, waits for them, and re-layouts: 1.92 us -> 0.04 us
  Pallas kernels: 3.97 us -> 3.17 us
    all_to_all x2 -> x3, blocking collectives: 40.7 us -> 53.8 us  [exchanged(): return lax.all_to_all(x, axes, 0, 0, tiled=True, axis_index_groups=[ranks])]
    all_to_all x1 -> x0, starting transfers between devices: 7.23 us -> none  [exchanged(): return lax.all_to_all(x, axes, 0, 0, tiled=True, axis_index_groups=[ranks])]
    all_to_all x1 -> x0, waiting for transfers between devices: 7.14 us -> none  [exchanged(): return lax.all_to_all(x, axes, 0, 0, tiled=True, axis_index_groups=[ranks])]
    ppermute x1, starting transfers between devices: 0.65 us -> 3.1 us  [device_step(): lax.ppermute(new_token, (HI, TP), token_route(far, lax.axis_size(TP)))]
    unnamed x18 -> x16, local copies, waits for them, and re-layouts: 1.92 us -> 0.04 us
    pallas_call x5, Pallas kernels: 3.97 us -> 3.17 us  [the longest x1 1.83 us: device_step(): pl.pallas_call(functools.partial(state_kernel, near_ranks), out_shape=sha...]
  transfers between devices with their start and end apart: 2 -> 1, of which waited for: 1 -> 1; matrix products, arithmetic and copies ran while one was open for 0% -> 0% of each run, Pallas kernels for 0% -> 3%
where the time goes in v9:
time: 61.4 us; the launch traced here: 61.2 us
  blocking collectives  53.8 us (88%)
  Pallas kernels  3.17 us (5%)
  starting transfers between devices  3.1 us (5%)
  between operations  0.77 us (1%)
    all_to_all x3, blocking collectives, exchanged(): return lax.all_to_all(x, axes, 0, 0, tiled=True, axis_index_groups=[ranks])  53.8 us
    ppermute x1, starting transfers between devices, device_step(): lax.ppermute(new_token, (HI, TP), token_route(far, lax.axis_size(TP)))  3.1 us
    pallas_call x1, Pallas kernels, device_step(): pl.pallas_call(functools.partial(state_kernel, near_ranks), out_shape=sha...  1.83 us
  transfers between devices with their start and end apart: 1, of which 1 were waited for; matrix products, arithmetic and copies ran while one was open for 0% of the time, Pallas kernels for 3%

profile of v9, /device:TPU:2, one launch (start us, length us, event | category | flops | bytes accessed | tf_op | source)
XLA Modules:
  0.0 61.2 jit_solution(1943598899314401033)
XLA Ops:
  0.6 0.0 copy-start.2
  0.6 0.0 copy-start.1
  0.7 0.0 copy-start.6
  0.7 0.0 copy-start.5
  0.7 0.0 copy-start
  0.7 3.1 %collective-permute-start = (bf16[8,256]{1,0:T(8,128)(2,1)}, bf16[8,256]{1,0:T(8,128)(2,1)S(1)}, u32[]{:S(2)}, u32[]{:S(2)}) collective-permute-start(bf16[8,256]{1,0:T(8,128)(2,1)} %param.11), channel_id=1, source_target_pairs={{7,0},{6,1},{5,2},{4,3},{3,4},{2,5},{1,6},{0,7},{70,64},{71,65},{6... | collective-permute-start | bytes 12296 | tf_op jit(solution)/shard_map/ppermute | solution.py:203
  3.8 0.0 copy-done.2
  3.8 0.0 copy-done.1
  3.8 0.0 copy-done.6
  3.8 0.0 copy-done.5
  3.8 0.0 copy-done
  3.9 0.0 copy-start.3
  3.9 0.0 copy-start.4
  3.9 1.8 %block_states.1 = f32[8,136,128]{2,1,0:T(8,128)S(1)} custom-call(f32[8,128]{1,0:T(8,128)S(1)} %opening.1.opening_ref, bf16[8,64,2048]{2,1,0:T(8,128)(2,1)S(1)} %copy-done, f32[8,64]{1,0:T(8,128)S(1)} %copy-done.5, f32[1,128]{1,0:T(1,128)S(1)} %bitcast.7, bf16[2048,128]{1,0:T(8,128)(2,1)S(1)} %copy-done.1, bf16[2048,128]{1,0:T(8,128)(2,1)S(1)} %copy-done.2), custom_call_target="tpu_custom_call" | custom-call | flops 600000000 | bytes 4000000 | tf_op jit(solution)/shard_map/block_states/pallas_call | solution.py:204
  5.7 0.0 copy-start.7
  5.7 0.4 collective-permute-done.token_ref
  6.1 15.2 %all_to_all.15.in_ref = f32[8,136,128]{2,1,0:T(8,128)S(1)} all-to-all(f32[8,136,128]{2,1,0:T(8,128)S(1)} %block_states.1), channel_id=1, replica_groups={{16,0,24,8,48,32,56,40},{17,1,25,9,49,33,57,41},{18,2,26,10,50,34,58,42..., dimensions={0} | all-to-all | bytes 1114112 | tf_op jit(solution)/shard_map/all_to_all | solution.py:174
  21.2 0.0 copy-done.3
  21.2 0.0 copy-done.4
  21.2 0.4 near_states.1
  21.7 19.7 %all_to_all.16.in_ref = f32[8,24,128]{2,1,0:T(8,128)S(1)} all-to-all(f32[8,24,128]{2,1,0:T(8,128)S(1)} %near_states.1), channel_id=1, replica_groups={{256,0,448,64,384,128,320,192},{257,1,449,65,385,129,321,193},{258,2,45..., dimensions={0} | all-to-all | bytes 196608 | tf_op jit(solution)/shard_map/all_to_all | solution.py:174
  41.3 0.0 copy-done.7
  41.3 0.2 far_states.1
  41.6 19.0 %all_to_all.17 = f32[64,1,256]{2,1,0:T(1,128)S(1)} all-to-all(f32[64,1,256]{2,1,0:T(1,128)S(1)} %bitcast.6), channel_id=1, replica_groups={{272,256,280,264,304,288,312,296,16,0,24,8,48,32,56,40,464,448,472,456,..., dimensions={0} | all-to-all | bytes 131072 | tf_op jit(solution)/shard_map/all_to_all | solution.py:174
  60.5 0.7 %read.1 = (bf16[8,128]{1,0:T(8,128)(2,1)}, bf16[16,128]{1,0:T(8,128)(2,1)}) custom-call(f32[128,128]{1,0:T(8,128)S(1)} %bitcast.5, bf16[16,128]{1,0:T(8,128)(2,1)S(1)} %get-tuple-element.11.state_ref), custom_call_target="tpu_custom_call" | custom-call | flops 100000 | bytes 40000 | tf_op jit(solution)/shard_map/read/pallas_call | solution.py:238
  (1 shorter events, 0.0 us)
Async XLA Ops:
  0.6 3.2 %copy-start.2 = (bf16[2048,128]{1,0:T(8,128)(2,1)S(1)}, bf16[2048,128]{1,0:T(8,128)(2,1)}, u32[]{:S(2)}) copy-start(bf16[2048,128]{1,0:T(8,128)(2,1)} %wv_ref.3) | copy-start | bytes 1572868
  0.6 3.2 %copy-start.1 = (bf16[2048,128]{1,0:T(8,128)(2,1)S(1)}, bf16[2048,128]{1,0:T(8,128)(2,1)}, u32[]{:S(2)}) copy-start(bf16[2048,128]{1,0:T(8,128)(2,1)} %wf_ref.3) | copy-start | bytes 1572868
  0.7 3.2 %copy-start.6 = (f32[128]{0:T(128)S(1)}, f32[128]{0:T(128)}, u32[]{:S(2)}) copy-start(f32[128]{0:T(128)} %param.16) | copy-start | bytes 1540
  0.7 3.2 %copy-start.5 = (f32[8,64]{1,0:T(8,128)S(1)}, f32[8,64]{1,0:T(8,128)}, u32[]{:S(2)}) copy-start(f32[8,64]{1,0:T(8,128)} %keep_ref.1) | copy-start | bytes 6148
  0.7 3.2 %copy-start = (bf16[8,64,2048]{2,1,0:T(8,128)(2,1)S(1)}, bf16[8,64,2048]{2,1,0:T(8,128)(2,1)}, u32[]{:S(2)}) copy-start(bf16[8,64,2048]{2,1,0:T(8,128)(2,1)} %prompt_ref.1) | copy-start | bytes 6291460
  0.7 5.4 %collective-permute-start = (bf16[8,256]{1,0:T(8,128)(2,1)}, bf16[8,256]{1,0:T(8,128)(2,1)S(1)}, u32[]{:S(2)}, u32[]{:S(2)}) collective-permute-start(bf16[8,256]{1,0:T(8,128)(2,1)} %param.11), channel_id=1, source_target_pairs={{7,0},{6,1},{5,2},{4,3},{3,4},{2,5},{1,6},{0,7},{70,64},{71,65},{6... | collective-permute-start | bytes 12296 | tf_op jit(solution)/shard_map/ppermute | solution.py:203
  3.9 17.4 %copy-start.3 = (bf16[2048,128]{1,0:T(8,128)(2,1)S(1)}, bf16[2048,128]{1,0:T(8,128)(2,1)}, u32[]{:S(2)}) copy-start(bf16[2048,128]{1,0:T(8,128)(2,1)} %wq_ref.1) | copy-start | bytes 1572868
  3.9 17.4 %copy-start.4 = (bf16[2048,128]{1,0:T(8,128)(2,1)S(1)}, bf16[2048,128]{1,0:T(8,128)(2,1)}, u32[]{:S(2)}) copy-start(bf16[2048,128]{1,0:T(8,128)(2,1)} %wg_ref.1) | copy-start | bytes 1572868
  5.7 35.6 %copy-start.7 = (f32[128]{0:T(128)S(1)}, f32[128]{0:T(128)}, u32[]{:S(2)}) copy-start(f32[128]{0:T(128)} %param.17) | copy-start | bytes 1540
